TPU v7x, 256 devices: a whole 4x4x8 slice. The times are simulated.
256 devices in a mesh: ep: 16 (over y, x), tp: 16 (over z, core).
Axes of the slice: x: 4, y: 4, z: 8, core: 2. Of those that a mesh axis runs over, the one named last changes fastest.
Arguments:
- stream: bfloat16 [131072, 1024], P(('ep', 'tp')), may hold values from -6 to 6
- norm_gain: float32 [1024], replicated, may hold values from 0.5 to 1.5
- gate_rows: bfloat16 [16, 1024, 1024], P('ep', 'tp'), may hold values from -0.1875 to 0.1875
- up_rows: bfloat16 [16, 1024, 1024], P('ep', 'tp'), may hold values from -0.1875 to 0.1875
- down_rows: bfloat16 [16, 1024, 1024], P('ep', 'tp'), may hold values from -0.1875 to 0.1875
- chosen: int32 [16, 16384], P('ep'), may hold values from 0 to 131071, as said below
- affinity: float32 [16, 16384], P('ep'), may hold values from 0.2 to 1
Outputs:
- mixed_out: bfloat16 [131072, 1024], P(('ep', 'tp'))
Inputs may be any that keep to these rules, and one draw needn't show every extreme that they name: Each row of chosen names 16384 different token numbers in increasing order. Among the 512 consecutive token numbers of any one device, an expert reads at most 128, and for every expert some device holds exactly 128 of its tokens.
All inputs are finite; a program needn't handle non-finite values.
Results may differ from a plain program's by a relative error of at most 0.008.
Values may be sent and summed in bfloat16 or wider, within the bound.
No kernel may reach another device: no remote copies, remote signals or barrier semaphores. Data moves between devices by JAX's collectives and lax.ppermute only.
A program may use at most 64 MiB of HBM per device.

v0:
```python
import functools

import jax
import jax.numpy as jnp
from jax import lax
from jax.experimental import pallas as pl
from jax.experimental.pallas import tpu as pltpu
from jax.sharding import PartitionSpec as P

epsilon = 1e-06
SIDE = 4
SMEM = pl.BlockSpec(memory_space=pltpu.SMEM)
VMEM = pl.BlockSpec(memory_space=pltpu.VMEM)


def wrap(value):
    return lax.rem(value + SIDE, SIDE)


def windows_kernel(block, slots, bounds_ref, list_ref, affinity_ref, rows_ref, weights_ref):
    listed = list_ref[...]
    lines = listed.shape[0]
    lane = lax.broadcasted_iota(jnp.int32, (1, slots), 1)

    def cut(j, carry):
        y, x = j // SIDE, lax.rem(j, SIDE)
        bound = bounds_ref[j]
        start = jnp.sum((listed < bound).astype(jnp.int32))
        line, shift = start // slots, start % slots
        first = jnp.minimum(line, lines - 1)
        second = jnp.minimum(line + 1, lines - 1)
        back = lax.rem(slots - shift, slots)

        def window(ref):
            low = pltpu.roll(ref[pl.ds(first, 1), :], back, 1)
            high = pltpu.roll(ref[pl.ds(second, 1), :], back, 1)
            return jnp.where(lane < slots - shift, low, high)

        rows = window(list_ref) - bound
        rows = jnp.where((rows >= 0) & (rows < block), rows, -1)
        for t in range(SIDE):
            rows_ref[y * SIDE + wrap(x + t - SIDE), t : t + 1, :] = rows
            rows_ref[wrap(y + t - SIDE) * SIDE + x, SIDE + t : SIDE + t + 1, :] = rows
        weights_ref[pl.ds(j, 1), :] = window(affinity_ref)
        return carry

    lax.fori_loop(0, weights_ref.shape[0], cut, 0, unroll=4)


def windows(bounds, listed, affinity, block, slots):
    count = bounds.shape[0]
    return pl.pallas_call(
        functools.partial(windows_kernel, block, slots),
        in_specs=[SMEM, VMEM, VMEM],
        out_shape=(
            jax.ShapeDtypeStruct((count, 2 * SIDE, slots), jnp.int32),
            jax.ShapeDtypeStruct((count, slots), jnp.float32),
        ),
        cost_estimate=pl.CostEstimate(flops=8_000_000, bytes_accessed=150_000, transcendentals=0),
        name="windows",
    )(bounds, listed.reshape(-1, slots), affinity.reshape(-1, slots))


def prepare_kernel(stream_ref, gain_ref, gate_ref, up_ref, down_ref, low_ref, high_ref, piece_ref):
    values = stream_ref[...].astype(jnp.float32)
    inverse = lax.rsqrt(jnp.mean(values * values, axis=-1, keepdims=True) + epsilon)
    normed = (values * inverse * gain_ref[...]).astype(jnp.bfloat16)
    half = low_ref.shape[1]
    low_ref[...] = normed[:, :half]
    high_ref[...] = normed[:, half:]

    @pl.when(pl.program_id(0) == 0)
    def _():
        piece_ref[0:1] = gate_ref[...]
        piece_ref[1:2] = up_ref[...]
        piece_ref[2:3] = down_ref[...]


def prepare(stream, norm_gain, parts):
    rows, features = stream.shape
    step, half = rows // 2, features // 2
    part = pl.BlockSpec(parts[0].shape, lambda i: (0, 0, 0))
    piece = (3, *parts[0].shape[1:])
    return pl.pallas_call(
        prepare_kernel,
        grid=(2,),
        in_specs=[
            pl.BlockSpec((step, features), lambda i: (i, 0)),
            pl.BlockSpec((1, features), lambda i: (0, 0)),
            part,
            part,
            part,
        ],
        out_specs=(
            pl.BlockSpec((step, half), lambda i: (i, 0)),
            pl.BlockSpec((step, half), lambda i: (i, 0)),
            pl.BlockSpec(piece, lambda i: (0, 0, 0)),
        ),
        out_shape=(
            jax.ShapeDtypeStruct((rows, half), jnp.bfloat16),
            jax.ShapeDtypeStruct((rows, half), jnp.bfloat16),
            jax.ShapeDtypeStruct(piece, jnp.bfloat16),
        ),
        cost_estimate=pl.CostEstimate(flops=3_000_000, bytes_accessed=3 << 20, transcendentals=512),
        name="prepare",
    )(stream, norm_gain.reshape(1, features), *parts)


def pick_kernel(along_y, place_ref, rows_ref, own_ref, after_ref, top_ref, bottom_ref, before_ref, *refs):
    outs = refs[:SIDE]
    across_ref, chosen_ref = refs[SIDE:]
    y, x = place_ref[0], place_ref[1]
    tokens, half = own_ref.shape
    slots = rows_ref.shape[2]
    across_ref[: tokens // 2, :] = top_ref[...]
    across_ref[tokens // 2 :, :] = bottom_ref[...]
    token = lax.broadcasted_iota(jnp.int32, (slots, tokens), 1).astype(jnp.float32)
    for d in range(SIDE):
        e = wrap(y + d) * SIDE + x if along_y else y * SIDE + wrap(x + d)
        column = rows_ref[e].astype(jnp.float32).T
        for t in range(SIDE):
            k = t if along_y else SIDE + t
            chosen_ref[t, d * slots : (d + 1) * slots, :] = jnp.where(column[:, k : k + 1] == token, 1.0, 0.0).astype(
                jnp.bfloat16
            )
    step = half // 2

    def work(i, carry):
        at = pl.ds(pl.multiple_of(i * step, step), step)
        for t, source in enumerate((own_ref, after_ref, across_ref, before_ref)):
            rows = jnp.dot(chosen_ref[t], source[:, at], preferred_element_type=jnp.float32).astype(jnp.bfloat16)
            for d in range(SIDE):
                outs[d][t * slots : (t + 1) * slots, at] = rows[d * slots : (d + 1) * slots, :]
        return carry

    lax.fori_loop(0, 2, work, 0)


def pick(along_y, place, rows, sources):
    tokens, half = sources[0].shape
    slots = rows.shape[2]
    return pl.pallas_call(
        functools.partial(pick_kernel, along_y),
        in_specs=[SMEM] + [VMEM] * 6,
        out_shape=[jax.ShapeDtypeStruct((SIDE * slots, half), jnp.bfloat16)] * SIDE,
        scratch_shapes=[
            pltpu.VMEM((tokens, half), jnp.bfloat16),
            pltpu.VMEM((SIDE, SIDE * slots, tokens), jnp.bfloat16),
        ],
        cost_estimate=pl.CostEstimate(
            flops=2 * SIDE * SIDE * slots * tokens * half, bytes_accessed=4 << 20, transcendentals=0
        ),
        compiler_params=pltpu.CompilerParams(vmem_limit_bytes=14 << 20),
        name="pick_y" if along_y else "pick_x",
    )(place, rows, *sources)


def stack_kernel(*refs):
    out_ref, at = refs[-1], 0
    for piece in refs[:-1]:
        width = piece.shape[1]
        out_ref[:, at : at + width, :] = piece[...]
        at += width


def stack(pieces):
    return pl.pallas_call(
        stack_kernel,
        in_specs=[VMEM] * len(pieces),
        out_shape=jax.ShapeDtypeStruct(
            (3, sum(piece.shape[1] for piece in pieces), pieces[0].shape[2]), jnp.bfloat16
        ),
        cost_estimate=pl.CostEstimate(flops=1_000_000, bytes_accessed=4 << 20, transcendentals=0),
        compiler_params=pltpu.CompilerParams(vmem_limit_bytes=8 << 20),
    )(*pieces)


def assemble_kernel(*refs):
    pieces, outs = refs[:-3], refs[-3:]
    step = 64
    at = 0
    for piece in pieces:
        width = piece.shape[1]
        for j, out in enumerate(outs):

            def move(i, carry, piece=piece, out=out, j=j, at=at):
                rows = pl.multiple_of(i * step, step)
                out[pl.ds(at + rows, step), :] = piece[j, pl.ds(rows, step), :]
                return carry

            lax.fori_loop(0, width // step, move, 0)
        at += width


def assemble(pieces):
    shape = jax.ShapeDtypeStruct((sum(piece.shape[1] for piece in pieces), pieces[0].shape[2]), jnp.bfloat16)
    return pl.pallas_call(
        assemble_kernel,
        in_specs=[VMEM] * len(pieces),
        out_shape=[shape] * 3,
        cost_estimate=pl.CostEstimate(flops=1_000_000, bytes_accessed=12 << 20, transcendentals=0),
        compiler_params=pltpu.CompilerParams(vmem_limit_bytes=16 << 20),
        name="assemble",
    )(*pieces)


STEPS = (
    ((2, 0), (2, 1), (2, 2), (2, 3), (0, 2), (1, 2), (3, 2), (1, 1)),
    ((1, 0), (1, 3), (0, 1), (3, 1), (3, 0), (3, 3), (0, 3), (0, 0)),
)
FINISHED = (
    (("low", 2), ("high", 2)),
    (("low", 1), ("high", 1), ("low", 3), ("high", 3), ("low", 0), ("high", 0)),
)


def members(piece):
    half, fixed = piece
    return [(fixed, k) if half == "low" else (k, fixed) for k in range(SIDE)]


def expert_kernel(number, names, place_ref, weights_ref, gate_ref, up_ref, down_ref, *refs):
    inputs_ref, result_ref, columns_ref = refs[-3:]
    ref = dict(zip(names, refs))
    blocks = STEPS[number]
    y, x = place_ref[0], place_ref[1]
    slots, half = weights_ref.shape[1], ref["in", "low", blocks[0][0]].shape[1]
    for k, (a, b) in enumerate(blocks):
        at = slice(k * slots, (k + 1) * slots)
        inputs_ref[at, :half] = ref["in", "low", a][b * slots : (b + 1) * slots, :]
        inputs_ref[at, half:] = ref["in", "high", b][a * slots : (a + 1) * slots, :]
        line = weights_ref[pl.ds(wrap(y - a) * SIDE + wrap(x - b), 1), :]
        columns_ref[at, :] = jnp.broadcast_to(line, (slots, slots)).T
    last = (((1,), (1,)), ((), ()))
    units = gate_ref.shape[0]
    width, rows = units // 4, SIDE * slots

    def work(i, carry):
        at = pl.ds(pl.multiple_of(i * rows, rows), rows)
        inputs = inputs_ref[at, :]
        hidden = []
        for f in range(0, units, width):
            gate_sum = lax.dot_general(inputs, gate_ref[f : f + width, :], last, preferred_element_type=jnp.float32)
            up_sum = lax.dot_general(inputs, up_ref[f : f + width, :], last, preferred_element_type=jnp.float32)
            hidden.append((gate_sum / (1.0 + jnp.exp(-gate_sum)) * up_sum).astype(jnp.bfloat16))
        result = jnp.dot(jnp.concatenate(hidden, 1), down_ref[...], preferred_element_type=jnp.float32)
        result_ref[at, :] = (result * columns_ref[at, :][:, :1]).astype(jnp.bfloat16)
        return carry

    lax.fori_loop(0, len(blocks) // SIDE, work, 0)

    def part(block, which):
        if block in blocks:
            k = blocks.index(block)
            cut = slice(0, half) if which == "low" else slice(half, 2 * half)
            return result_ref[k * slots : (k + 1) * slots, cut]
        step = next(n for n in range(number) if block in STEPS[n])
        k = STEPS[step].index(block)
        return ref["made", which, step][k * slots : (k + 1) * slots, :]

    for name in names:
        if name[0] == "out":
            for k, block in enumerate(members(name[1:])):
                ref[name][k * slots : (k + 1) * slots, :] = part(block, name[1])
        if name == ("made", name[1], number):
            for k, block in enumerate(blocks):
                ref[name][k * slots : (k + 1) * slots, :] = part(block, name[1])


def expert(number, place, weights, projections, low, high, made):
    slots, half = weights.shape[1], low[0].shape[1]
    features, units = 2 * half, projections[0].shape[0]
    piece_rows = SIDE * slots
    blocks = STEPS[number]
    total = len(blocks) * slots
    inputs = {("in", "low", a): low[a] for a, _ in blocks}
    inputs.update({("in", "high", b): high[b] for _, b in blocks})
    for piece in FINISHED[number]:
        for block in members(piece):
            step = next(n for n in range(len(STEPS)) if block in STEPS[n])
            if step < number:
                inputs["made", piece[0], step] = made[piece[0], step]
    outs = [("out", *piece) for piece in FINISHED[number]]
    for which in ("low", "high"):
        later = [
            piece
            for done in FINISHED[number + 1 :]
            for piece in done
            if piece[0] == which and any(block in blocks for block in members(piece))
        ]
        if later:
            outs.append(("made", which, number))
    shapes = [(piece_rows if name[0] == "out" else total, half) for name in outs]
    results = pl.pallas_call(
        functools.partial(expert_kernel, number, [*inputs, *outs]),
        in_specs=[SMEM] + [VMEM] * (4 + len(inputs)),
        out_shape=[jax.ShapeDtypeStruct(shape, jnp.bfloat16) for shape in shapes],
        scratch_shapes=[
            pltpu.VMEM((total, features), jnp.bfloat16),
            pltpu.VMEM((total, features), jnp.bfloat16),
            pltpu.VMEM((total, slots), jnp.float32),
        ],
        cost_estimate=pl.CostEstimate(
            flops=6 * total * units * features, bytes_accessed=4 * total * features, transcendentals=2 * total * units
        ),
        compiler_params=pltpu.CompilerParams(vmem_limit_bytes=28 << 20),
    )(place, weights, *projections, *inputs.values())
    results = dict(zip(outs, results))
    made.update({name[1:]: array for name, array in results.items() if name[0] == "made"})
    return {name[1:]: array for name, array in results.items() if name[0] == "out"}


def relay_kernel(place_ref, rows_ref, *refs):
    y, x = place_ref[0], place_ref[1]
    tokens, slots = refs[-1].shape[0], rows_ref.shape[2]
    step = tokens // 2
    token = lax.broadcasted_iota(jnp.int32, (step, slots), 0)
    for along_y in (True, False):
        first = 0 if along_y else SIDE
        pieces, outs = refs[first : first + SIDE], refs[first + 2 * SIDE : first + 3 * SIDE]
        lists = [rows_ref[wrap(y + d) * SIDE + x if along_y else y * SIDE + wrap(x + d)] for d in range(SIDE)]

        def work(i, carry, first=first, pieces=pieces, outs=outs, lists=lists):
            for t in range(SIDE):
                k = first + t
                chosen = jnp.concatenate(
                    [
                        jnp.where(token + i * step == rows[k : k + 1, :], 1.0, 0.0).astype(jnp.bfloat16)
                        for rows in lists
                    ],
                    1,
                )
                rows = jnp.concatenate([piece[t * slots : (t + 1) * slots, :] for piece in pieces])
                total = jnp.dot(chosen, rows, preferred_element_type=jnp.float32)
                outs[t][pl.ds(pl.multiple_of(i * step, step), step), :] = total.astype(jnp.bfloat16)
            return carry

        lax.fori_loop(0, 2, work, 0)


def relay(place, rows, lows, highs, tokens):
    total, half = lows[0].shape
    return pl.pallas_call(
        relay_kernel,
        in_specs=[SMEM] + [VMEM] * (1 + len(lows) + len(highs)),
        out_shape=[jax.ShapeDtypeStruct((tokens, half), jnp.bfloat16)] * (2 * SIDE),
        cost_estimate=pl.CostEstimate(
            flops=4 * SIDE * total * tokens * half, bytes_accessed=8 << 20, transcendentals=0
        ),
        compiler_params=pltpu.CompilerParams(vmem_limit_bytes=16 << 20),
        name="relay",
    )(place, rows, *lows, *highs)


def add_kernel(*refs):
    out_ref = refs[-1]
    half = refs[0].shape[1]
    for n, parts in enumerate((refs[:SIDE], refs[SIDE : 2 * SIDE])):
        total = parts[0][...].astype(jnp.float32)
        for part in parts[1:]:
            total = total + part[...].astype(jnp.float32)
        out_ref[:, n * half : (n + 1) * half] = total.astype(jnp.bfloat16)


def add(lows, highs):
    tokens, half = lows[0].shape
    step = tokens // 4
    return pl.pallas_call(
        add_kernel,
        grid=(4,),
        in_specs=[pl.BlockSpec((step, half), lambda i: (i, 0))] * (2 * SIDE),
        out_specs=pl.BlockSpec((step, 2 * half), lambda i: (i, 0)),
        out_shape=jax.ShapeDtypeStruct((tokens, 2 * half), jnp.bfloat16),
        cost_estimate=pl.CostEstimate(flops=4_000_000, bytes_accessed=5 << 20, transcendentals=0),
        compiler_params=pltpu.CompilerParams(vmem_limit_bytes=12 << 20),
        name="add",
    )(*lows, *highs)


def over_plane(array, by_y, by_x):
    places = [(y, x) for y in range(SIDE) for x in range(SIDE)]
    return lax.ppermute(
        array, "ep", [(y * SIDE + x, (y + by_y) % SIDE * SIDE + (x + by_x) % SIDE) for y, x in places]
    )


def along_z(array, by, tp_count):
    chips = tp_count // 2
    pairs = [(z, c, (z + (-by if c else by)) % chips) for z in range(chips) for c in range(2)]
    return lax.ppermute(array, "tp", [(z * 2 + c, to * 2 + c) for z, c, to in pairs])


def other_core(array, tp_count):
    return lax.ppermute(array, "tp", [(j, j ^ 1) for j in range(tp_count)])


def layer(stream, norm_gain, gate_rows, up_rows, down_rows, chosen, affinity):
    ep_count = lax.axis_size("ep")
    tp_count = lax.axis_size("tp")
    block, _ = stream.shape
    slots = 4 * block // ep_count
    ep_index = lax.axis_index("ep").astype(jnp.int32)
    place = jnp.stack([ep_index // SIDE, ep_index % SIDE])
    bounds = (jnp.arange(ep_count, dtype=jnp.int32) * tp_count + lax.axis_index("tp")) * block
    low, high, own = prepare(stream, norm_gain, (gate_rows, up_rows, down_rows))
    left, right = over_plane(low, 0, 1), over_plane(low, 0, -1)
    down, up = over_plane(high, 1, 0), over_plane(high, -1, 0)
    both = stack([own, other_core(own, tp_count)])
    next1 = along_z(both, 1, tp_count)
    rows_there, weights = windows(bounds, chosen, affinity, block, slots)
    rows_here = lax.all_to_all(rows_there, "ep", split_axis=0, concat_axis=0, tiled=True)
    mid = block // 2
    lows = [low, left, over_plane(left[:mid], 0, 1), over_plane(right[mid:], 0, -1), right]
    highs = [high, down, over_plane(down[:mid], 1, 0), over_plane(up[mid:], -1, 0), up]
    next2 = along_z(next1, 1, tp_count)
    picked_low = pick(True, place, rows_here, lows)
    arrived_low = [picked_low[0]] + [over_plane(picked_low[d], d, 0) for d in range(1, SIDE)]
    next3 = along_z(next2, 1, tp_count)
    picked_high = pick(False, place, rows_here, highs)
    arrived_high = [picked_high[0]] + [over_plane(picked_high[d], 0, d) for d in range(1, SIDE)]
    across = along_z(next2[:, : own.shape[1]], 2, tp_count)
    held = [next1, next2, next3, across]
    pieces = [both, *held, *(other_core(piece, tp_count) for piece in held)]
    projections = assemble(pieces)
    made, back = {}, {}
    for number in range(len(STEPS)):
        finished = expert(number, place, weights, projections, arrived_low, arrived_high, made)
        for (half, by), piece in finished.items():
            if by == 0:
                back[half, by] = piece
            elif half == "low":
                back[half, by] = over_plane(piece, -by, 0)
            else:
                back[half, by] = over_plane(piece, 0, -by)
    lows, highs = [back["low", d] for d in range(SIDE)], [back["high", d] for d in range(SIDE)]
    sums = relay(place, rows_here, lows, highs, block)
    lows, highs = [sums[0]], [sums[SIDE]]
    for t in (1, 3, 2):
        lows.append(over_plane(sums[t], 0, -t))
        highs.append(over_plane(sums[SIDE + t], -t, 0))
    return add(lows, highs)


def solution(mesh):
    return jax.shard_map(
        layer,
        mesh=mesh,
        in_specs=(
            P(("ep", "tp"), None),
            P(),
            P("ep", "tp", None),
            P("ep", "tp", None),
            P("ep", "tp", None),
            P("ep", None),
            P("ep", None),
        ),
        out_specs=P(("ep", "tp"), None),
        check_vma=False,
    )
```

profile of v0, /device:TPU:30, one launch (start us, length us, event | category | flops | bytes accessed | tf_op | source)
XLA Modules:
  0.0 201.4 jit_solution(3544199571778860157)
XLA Ops:
  0.0 2.6 %prepare.1 = (bf16[512,512]{1,0:T(8,128)(2,1)}, bf16[512,512]{1,0:T(8,128)(2,1)}, bf16[3,64,1024]{2,1,0:T(8,128)(2,1)}) custom-call(bf16[512,1024]{1,0:T(8,128)(2,1)} %stream_ref.1, f32[1,1024]{1,0:T(1,128)} %bitcast.7, bf16[1,64,1024]{2,1,0:T(8,128)(2,1)} %gate_ref.1, bf16[1,64,1024]{2,1,0:T(8,128)(2,1)} %up_ref.1, bf16[1,64,1024]{2,1,0:T(8,128)(2,1)} %down_ref.1), custom_call_target="tpu_custom_call" | custom-call | flops 3000000 | bytes 3145728 | tf_op jit(solution)/shard_map/prepare/pallas_call | solution.py:84
  7.7 13.9 %collective-permute-done.1.refs_1_ = bf16[3,128,1024]{2,1,0:T(8,128)(2,1)S(1)} collective-permute-done((bf16[3,128,1024]{2,1,0:T(8,128)(2,1)S(1)}, bf16[3,128,1024]{2,1,0:T(8,128)(2,1)S(1)}, u32[]{:S(2)}, u32[]{:S(2)}) %collective-permute-start.1) | collective-permute-done | bytes 786464 | tf_op jit(solution)/shard_map/ppermute | solution.py:390
  23.8 10.9 %collective-permute-done.2.refs_2_ = bf16[3,128,1024]{2,1,0:T(8,128)(2,1)S(1)} collective-permute-done((bf16[3,128,1024]{2,1,0:T(8,128)(2,1)S(1)}, bf16[3,128,1024]{2,1,0:T(8,128)(2,1)S(1)}, u32[]{:S(2)}, u32[]{:S(2)}) %collective-permute-start.2) | collective-permute-done | bytes 786464 | tf_op jit(solution)/shard_map/ppermute | solution.py:390
  43.1 7.9 %collective-permute-done.17.before_ref = bf16[512,512]{1,0:T(8,128)(2,1)} collective-permute-done((bf16[512,512]{1,0:T(8,128)(2,1)}, bf16[512,512]{1,0:T(8,128)(2,1)}, u32[]{:S(2)}, u32[]{:S(2)}) %collective-permute-start.17) | collective-permute-done | bytes 524320 | tf_op jit(solution)/shard_map/ppermute | solution.py:382
  58.0 7.6 %all-to-all-start = ((s32[16,8,128]{2,1,0:T(8,128)}), s32[16,8,128]{2,1,0:T(8,128)}, u32[]{:S(2)}, u32[]{:S(2)}) async-start(s32[16,8,128]{2,1,0:T(8,128)} %get-tuple-element.39), calls=%async_computation | async-start | bytes 131072 | tf_op jit(solution)/shard_map/all_to_all | solution.py:411
  65.7 4.2 %all-to-all-done.rows_ref = s32[16,8,128]{2,1,0:T(8,128)} async-done(((s32[16,8,128]{2,1,0:T(8,128)}), s32[16,8,128]{2,1,0:T(8,128)}, u32[]{:S(2)}, u32[]{:S(2)}) %all-to-all-start) | async-done | bytes 65568 | tf_op jit(solution)/shard_map/all_to_all | solution.py:411
  74.0 3.1 %pick_y.1 = (bf16[512,512]{1,0:T(8,128)(2,1)S(1)}, bf16[512,512]{1,0:T(8,128)(2,1)S(1)}, bf16[512,512]{1,0:T(8,128)(2,1)S(1)}, bf16[512,512]{1,0:T(8,128)(2,1)S(1)}) custom-call(s32[2]{0:T(128)S(1)} %pad_add_fusion.place_ref, s32[16,8,128]{2,1,0:T(8,128)} %all-to-all-done.rows_ref, bf16[512,512]{1,0:T(8,128)(2,1)S(1)} %copy-done.8, ...), custom_call_target="tpu_custom_call" | custom-call | flops 1073741824 | bytes 4194304 | tf_op jit(solution)/shard_map/pick_y/pallas_call | solution.py:142
  79.2 3.2 %pick_x.1 = (bf16[512,512]{1,0:T(8,128)(2,1)S(1)}, bf16[512,512]{1,0:T(8,128)(2,1)S(1)}, bf16[512,512]{1,0:T(8,128)(2,1)S(1)}, bf16[512,512]{1,0:T(8,128)(2,1)S(1)}) custom-call(s32[2]{0:T(128)S(1)} %pad_add_fusion.place_ref, s32[16,8,128]{2,1,0:T(8,128)} %all-to-all-done.rows_ref, bf16[512,512]{1,0:T(8,128)(2,1)S(1)} %copy-done.7, ...), custom_call_target="tpu_custom_call" | custom-call | flops 1073741824 | bytes 4194304 | tf_op jit(solution)/shard_map/pick_x/pallas_call | solution.py:142
  82.5 7.6 %collective-permute-done.13.refs_2_.refs_0_ = bf16[512,512]{1,0:T(8,128)(2,1)S(1)} collective-permute-done((bf16[512,512]{1,0:T(8,128)(2,1)S(1)}, bf16[512,512]{1,0:T(8,128)(2,1)S(1)}, u32[]{:S(2)}, u32[]{:S(2)}) %collective-permute-start.13) | collective-permute-done | bytes 524320 | tf_op jit(solution)/shard_map/ppermute | solution.py:382
  94.1 3.9 %collective-permute-start.21 = (bf16[512,512]{1,0:T(8,128)(2,1)S(1)}, bf16[512,512]{1,0:T(8,128)(2,1)S(1)}, u32[]{:S(2)}, u32[]{:S(2)}) collective-permute-start(bf16[512,512]{1,0:T(8,128)(2,1)S(1)} %get-tuple-element.53), channel_id=1, source_target_pairs={{0,128},{16,144},{32,160},{48,176},{64,192},{80,208},{96,224},{112... | collective-permute-start | bytes 1572872 | tf_op jit(solution)/shard_map/ppermute | solution.py:382
  101.0 4.2 %collective-permute-done.14.refs_3_.refs_2_ = bf16[512,512]{1,0:T(8,128)(2,1)S(1)} collective-permute-done((bf16[512,512]{1,0:T(8,128)(2,1)S(1)}, bf16[512,512]{1,0:T(8,128)(2,1)S(1)}, u32[]{:S(2)}, u32[]{:S(2)}) %collective-permute-start.14) | collective-permute-done | bytes 524320 | tf_op jit(solution)/shard_map/ppermute | solution.py:382
  106.6 8.0 %collective-permute-done.20.refs_5_ = bf16[512,512]{1,0:T(8,128)(2,1)S(1)} collective-permute-done((bf16[512,512]{1,0:T(8,128)(2,1)S(1)}, bf16[512,512]{1,0:T(8,128)(2,1)S(1)}, u32[]{:S(2)}, u32[]{:S(2)}) %collective-permute-start.20) | collective-permute-done | bytes 524320 | tf_op jit(solution)/shard_map/ppermute | solution.py:382
  116.0 8.0 %shard_map.74 = (bf16[512,512]{1,0:T(8,128)(2,1)S(1)}, bf16[512,512]{1,0:T(8,128)(2,1)S(1)}, bf16[1024,512]{1,0:T(8,128)(2,1)S(1)}, bf16[1024,512]{1,0:T(8,128)(2,1)S(1)}) custom-call(s32[2]{0:T(128)S(1)} %pad_add_fusion.place_ref, f32[16,128]{1,0:T(8,128)S(1)} %copy-done.11, bf16[1024,1024]{1,0:T(8,128)(2,1)S(1)} %get-tuple-element.42.gate_ref, ...), custom_call_target="tpu_custom_call" | custom-call | flops 6442450944 | bytes 4194304 | tf_op jit(solution)/shard_map/pallas_call | solution.py:294
  124.0 8.0 %shard_map.75 = (bf16[512,512]{1,0:T(8,128)(2,1)S(1)}, bf16[512,512]{1,0:T(8,128)(2,1)S(1)}, bf16[512,512]{1,0:T(8,128)(2,1)S(1)}, bf16[512,512]{1,0:T(8,128)(2,...) custom-call(s32[2]{0:T(128)S(1)} %pad_add_fusion.place_ref, f32[16,128]{1,0:T(8,128)S(1)} %copy-done.11, ...), custom_call_target="tpu_custom_call" | custom-call | flops 6442450944 | bytes 4194304 | tf_op jit(solution)/shard_map/pallas_call | solution.py:294
  132.4 3.0 %collective-permute-start.24 = (bf16[512,512]{1,0:T(8,128)(2,1)S(1)}, bf16[512,512]{1,0:T(8,128)(2,1)S(1)}, u32[]{:S(2)}, u32[]{:S(2)}) collective-permute-start(bf16[512,512]{1,0:T(8,128)(2,1)S(1)} %get-tuple-element.59), channel_id=1, source_target_pairs={{0,128},{16,144},{32,160},{48,176},{64,192},{80,208},{96,224},{112... | collective-permute-start | bytes 1572872 | tf_op jit(solution)/shard_map/ppermute | solution.py:382
  139.0 3.2 %collective-permute-start.27 = (bf16[512,512]{1,0:T(8,128)(2,1)S(1)}, bf16[512,512]{1,0:T(8,128)(2,1)S(1)}, u32[]{:S(2)}, u32[]{:S(2)}) collective-permute-start(bf16[512,512]{1,0:T(8,128)(2,1)S(1)} %get-tuple-element.63), channel_id=1, source_target_pairs={{0,32},{16,48},{32,0},{48,16},{64,96},{80,112},{96,64},{112,80},{1... | collective-permute-start | bytes 1572872 | tf_op jit(solution)/shard_map/ppermute | solution.py:382
  142.2 6.1 %collective-permute-done.23.refs_1_ = bf16[512,512]{1,0:T(8,128)(2,1)S(1)} collective-permute-done((bf16[512,512]{1,0:T(8,128)(2,1)S(1)}, bf16[512,512]{1,0:T(8,128)(2,1)S(1)}, u32[]{:S(2)}, u32[]{:S(2)}) %collective-permute-start.23) | collective-permute-done | bytes 524320 | tf_op jit(solution)/shard_map/ppermute | solution.py:382
  150.2 5.6 %collective-permute-done.24.refs_2_ = bf16[512,512]{1,0:T(8,128)(2,1)S(1)} collective-permute-done((bf16[512,512]{1,0:T(8,128)(2,1)S(1)}, bf16[512,512]{1,0:T(8,128)(2,1)S(1)}, u32[]{:S(2)}, u32[]{:S(2)}) %collective-permute-start.24) | collective-permute-done | bytes 524320 | tf_op jit(solution)/shard_map/ppermute | solution.py:382
  156.4 4.3 %collective-permute-done.27.refs_6_ = bf16[512,512]{1,0:T(8,128)(2,1)S(1)} collective-permute-done((bf16[512,512]{1,0:T(8,128)(2,1)S(1)}, bf16[512,512]{1,0:T(8,128)(2,1)S(1)}, u32[]{:S(2)}, u32[]{:S(2)}) %collective-permute-start.27) | collective-permute-done | bytes 524320 | tf_op jit(solution)/shard_map/ppermute | solution.py:382
  160.7 5.0 %collective-permute-done.28.refs_7_ = bf16[512,512]{1,0:T(8,128)(2,1)S(1)} collective-permute-done((bf16[512,512]{1,0:T(8,128)(2,1)S(1)}, bf16[512,512]{1,0:T(8,128)(2,1)S(1)}, u32[]{:S(2)}, u32[]{:S(2)}) %collective-permute-start.28) | collective-permute-done | bytes 524320 | tf_op jit(solution)/shard_map/ppermute | solution.py:382
  165.7 3.7 %relay.1 = (bf16[512,512]{1,0:T(8,128)(2,1)S(1)}, bf16[512,512]{1,0:T(8,128)(2,1)S(1)}, bf16[512,512]{1,0:T(8,128)(2,1)S(1)}, bf16[512,512]{1,0:T(8,128)(2,1)S(1...) custom-call(s32[2]{0:T(128)S(1)} %pad_add_fusion.place_ref, ...), custom_call_target="tpu_custom_call" | custom-call | flops 2147483648 | bytes 8388608 | tf_op jit(solution)/shard_map/relay/pallas_call | solution.py:343
  173.2 3.2 %collective-permute-start.33 = (bf16[512,512]{1,0:T(8,128)(2,1)S(1)}, bf16[512,512]{1,0:T(8,128)(2,1)S(1)}, u32[]{:S(2)}, u32[]{:S(2)}) collective-permute-start(bf16[512,512]{1,0:T(8,128)(2,1)S(1)} %get-tuple-element.71), channel_id=1, source_target_pairs={{0,64},{16,80},{32,96},{48,112},{64,128},{80,144},{96,160},{112,17... | collective-permute-start | bytes 1572872 | tf_op jit(solution)/shard_map/ppermute | solution.py:382
  176.4 12.6 %collective-permute-done.29.refs_1_ = bf16[512,512]{1,0:T(8,128)(2,1)S(1)} collective-permute-done((bf16[512,512]{1,0:T(8,128)(2,1)S(1)}, bf16[512,512]{1,0:T(8,128)(2,1)S(1)}, u32[]{:S(2)}, u32[]{:S(2)}) %collective-permute-start.29) | collective-permute-done | bytes 524320 | tf_op jit(solution)/shard_map/ppermute | solution.py:382
  189.0 10.7 %collective-permute-done.34.refs_7_ = bf16[512,512]{1,0:T(8,128)(2,1)S(1)} collective-permute-done((bf16[512,512]{1,0:T(8,128)(2,1)S(1)}, bf16[512,512]{1,0:T(8,128)(2,1)S(1)}, u32[]{:S(2)}, u32[]{:S(2)}) %collective-permute-start.34) | collective-permute-done | bytes 524320 | tf_op jit(solution)/shard_map/ppermute | solution.py:382
  (89 shorter events, 50.9 us)
Async XLA Ops:
  5.7 15.9 %collective-permute-start.1 = (bf16[3,128,1024]{2,1,0:T(8,128)(2,1)S(1)}, bf16[3,128,1024]{2,1,0:T(8,128)(2,1)S(1)}, u32[]{:S(2)}, u32[]{:S(2)}) collective-permute-start(bf16[3,128,1024]{2,1,0:T(8,128)(2,1)S(1)} %shard_map.73.refs_0_), channel_id=1, source_target_pairs={{0,2},{1,15},{2,4},{3,1},{4,6},{5,3},{6,8},{7,5},{8,10},{9,7},{10,... | collective-permute-start | bytes 2359304 | tf_op jit(solution)/shard_map/ppermute | solution.py:390
  22.1 16.0 %collective-permute-start.11 = (bf16[512,512]{1,0:T(8,128)(2,1)}, bf16[512,512]{1,0:T(8,128)(2,1)S(1)}, u32[]{:S(2)}, u32[]{:S(2)}) collective-permute-start(bf16[512,512]{1,0:T(8,128)(2,1)} %get-tuple-element.45.own_ref), channel_id=1, source_target_pairs={{0,48},{16,0},{32,16},{48,32},{64,112},{80,64},{96,80},{112,96},{1... | collective-permute-start | bytes 1572872 | tf_op jit(solution)/shard_map/ppermute | solution.py:382
  34.8 20.0 %collective-permute-start.3 = (bf16[3,128,1024]{2,1,0:T(8,128)(2,1)S(1)}, bf16[3,128,1024]{2,1,0:T(8,128)(2,1)S(1)}, u32[]{:S(2)}, u32[]{:S(2)}) collective-permute-start(bf16[3,128,1024]{2,1,0:T(8,128)(2,1)S(1)} %collective-permute-done.2.refs_2_), channel_id=1, source_target_pairs={{0,2},{1,15},{2,4},{3,1},{4,6},{5,3},{6,8},{7,5},{8,10},{9,7},{10,... | collective-permute-start | bytes 2359304 | tf_op jit(solution)/shard_map/ppermute | solution.py:390
  34.8 16.2 %collective-permute-start.17 = (bf16[512,512]{1,0:T(8,128)(2,1)}, bf16[512,512]{1,0:T(8,128)(2,1)}, u32[]{:S(2)}, u32[]{:S(2)}) collective-permute-start(bf16[512,512]{1,0:T(8,128)(2,1)} %get-tuple-element.49.own_ref), channel_id=1, source_target_pairs={{0,192},{16,208},{32,224},{48,240},{64,0},{80,16},{96,32},{112,48}... | collective-permute-start | bytes 1572872 | tf_op jit(solution)/shard_map/ppermute | solution.py:382
  36.4 17.1 %collective-permute-start.10 = (bf16[256,512]{1,0:T(8,128)(2,1)}, bf16[256,512]{1,0:T(8,128)(2,1)S(1)}, u32[]{:S(2)}, u32[]{:S(2)}) collective-permute-start(bf16[256,512]{1,0:T(8,128)(2,1)} %slice.21), channel_id=1, source_target_pairs={{0,16},{16,32},{32,48},{48,0},{64,80},{80,96},{96,112},{112,64},{1... | collective-permute-start | bytes 786440 | tf_op jit(solution)/shard_map/ppermute | solution.py:382
  52.7 24.4 %collective-permute-start.18 = (bf16[256,512]{1,0:T(8,128)(2,1)}, bf16[256,512]{1,0:T(8,128)(2,1)}, u32[]{:S(2)}, u32[]{:S(2)}) collective-permute-start(bf16[256,512]{1,0:T(8,128)(2,1)} %slice.24), channel_id=1, source_target_pairs={{0,192},{16,208},{32,224},{48,240},{64,0},{80,16},{96,32},{112,48}... | collective-permute-start | bytes 786440 | tf_op jit(solution)/shard_map/ppermute | solution.py:382
  54.2 36.7 %collective-permute-start.5 = (bf16[3,128,1024]{2,1,0:T(8,128)(2,1)S(1)}, bf16[3,128,1024]{2,1,0:T(8,128)(2,1)}, u32[]{:S(2)}, u32[]{:S(2)}) collective-permute-start(bf16[3,128,1024]{2,1,0:T(8,128)(2,1)S(1)} %collective-permute-done.1.refs_1_), channel_id=1, source_target_pairs={{0,1},{1,0},{2,3},{3,2},{4,5},{5,4},{6,7},{7,6},{8,9},{9,8},{10,11... | collective-permute-start | bytes 2359304 | tf_op jit(solution)/shard_map/ppermute | solution.py:394
  54.3 24.9 %collective-permute-start.4 = (bf16[3,64,1024]{2,1,0:T(8,128)(2,1)}, bf16[3,64,1024]{2,1,0:T(8,128)(2,1)S(1)}, u32[]{:S(2)}, u32[]{:S(2)}) collective-permute-start(bf16[3,64,1024]{2,1,0:T(8,128)(2,1)} %slice.20), channel_id=1, source_target_pairs={{0,4},{1,13},{2,6},{3,15},{4,8},{5,1},{6,10},{7,3},{8,12},{9,5},{1... | collective-permute-start | bytes 1179656 | tf_op jit(solution)/shard_map/ppermute | solution.py:390
  54.3 37.3 %collective-permute-start.6 = (bf16[3,128,1024]{2,1,0:T(8,128)(2,1)S(1)}, bf16[3,128,1024]{2,1,0:T(8,128)(2,1)}, u32[]{:S(2)}, u32[]{:S(2)}) collective-permute-start(bf16[3,128,1024]{2,1,0:T(8,128)(2,1)S(1)} %collective-permute-done.2.refs_2_), channel_id=1, source_target_pairs={{0,1},{1,0},{2,3},{3,2},{4,5},{5,4},{6,7},{7,6},{8,9},{9,8},{10,11... | collective-permute-start | bytes 2359304 | tf_op jit(solution)/shard_map/ppermute | solution.py:394
  54.8 43.3 %collective-permute-start.7 = (bf16[3,128,1024]{2,1,0:T(8,128)(2,1)S(1)}, bf16[3,128,1024]{2,1,0:T(8,128)(2,1)}, u32[]{:S(2)}, u32[]{:S(2)}) collective-permute-start(bf16[3,128,1024]{2,1,0:T(8,128)(2,1)S(1)} %collective-permute-done.3.refs_3_), channel_id=1, source_target_pairs={{0,1},{1,0},{2,3},{3,2},{4,5},{5,4},{6,7},{7,6},{8,9},{9,8},{10,11... | collective-permute-start | bytes 2359304 | tf_op jit(solution)/shard_map/ppermute | solution.py:394
  91.6 23.0 %collective-permute-start.20 = (bf16[512,512]{1,0:T(8,128)(2,1)S(1)}, bf16[512,512]{1,0:T(8,128)(2,1)S(1)}, u32[]{:S(2)}, u32[]{:S(2)}) collective-permute-start(bf16[512,512]{1,0:T(8,128)(2,1)S(1)} %get-tuple-element.52), channel_id=1, source_target_pairs={{0,16},{16,32},{32,48},{48,0},{64,80},{80,96},{96,112},{112,64},{1... | collective-permute-start | bytes 1572872 | tf_op jit(solution)/shard_map/ppermute | solution.py:382
  94.1 21.9 %collective-permute-start.21 = (bf16[512,512]{1,0:T(8,128)(2,1)S(1)}, bf16[512,512]{1,0:T(8,128)(2,1)S(1)}, u32[]{:S(2)}, u32[]{:S(2)}) collective-permute-start(bf16[512,512]{1,0:T(8,128)(2,1)S(1)} %get-tuple-element.53), channel_id=1, source_target_pairs={{0,128},{16,144},{32,160},{48,176},{64,192},{80,208},{96,224},{112... | collective-permute-start | bytes 1572872 | tf_op jit(solution)/shard_map/ppermute | solution.py:382
  98.0 18.0 %collective-permute-start.22 = (bf16[512,512]{1,0:T(8,128)(2,1)S(1)}, bf16[512,512]{1,0:T(8,128)(2,1)S(1)}, u32[]{:S(2)}, u32[]{:S(2)}) collective-permute-start(bf16[512,512]{1,0:T(8,128)(2,1)S(1)} %get-tuple-element.54), channel_id=1, source_target_pairs={{0,32},{16,48},{32,0},{48,16},{64,96},{80,112},{96,64},{112,80},{1... | collective-permute-start | bytes 1572872 | tf_op jit(solution)/shard_map/ppermute | solution.py:382
  132.1 16.2 %collective-permute-start.23 = (bf16[512,512]{1,0:T(8,128)(2,1)S(1)}, bf16[512,512]{1,0:T(8,128)(2,1)S(1)}, u32[]{:S(2)}, u32[]{:S(2)}) collective-permute-start(bf16[512,512]{1,0:T(8,128)(2,1)S(1)} %get-tuple-element.58), channel_id=1, source_target_pairs={{0,192},{16,208},{32,224},{48,240},{64,0},{80,16},{96,32},{112,48}... | collective-permute-start | bytes 1572872 | tf_op jit(solution)/shard_map/ppermute | solution.py:382
  132.4 23.3 %collective-permute-start.24 = (bf16[512,512]{1,0:T(8,128)(2,1)S(1)}, bf16[512,512]{1,0:T(8,128)(2,1)S(1)}, u32[]{:S(2)}, u32[]{:S(2)}) collective-permute-start(bf16[512,512]{1,0:T(8,128)(2,1)S(1)} %get-tuple-element.59), channel_id=1, source_target_pairs={{0,128},{16,144},{32,160},{48,176},{64,192},{80,208},{96,224},{112... | collective-permute-start | bytes 1572872 | tf_op jit(solution)/shard_map/ppermute | solution.py:382
  135.5 20.9 %collective-permute-start.25 = (bf16[512,512]{1,0:T(8,128)(2,1)S(1)}, bf16[512,512]{1,0:T(8,128)(2,1)S(1)}, u32[]{:S(2)}, u32[]{:S(2)}) collective-permute-start(bf16[512,512]{1,0:T(8,128)(2,1)S(1)} %get-tuple-element.60), channel_id=1, source_target_pairs={{0,64},{16,80},{32,96},{48,112},{64,128},{80,144},{96,160},{112,17... | collective-permute-start | bytes 1572872 | tf_op jit(solution)/shard_map/ppermute | solution.py:382
  137.8 18.6 %collective-permute-start.26 = (bf16[512,512]{1,0:T(8,128)(2,1)S(1)}, bf16[512,512]{1,0:T(8,128)(2,1)S(1)}, u32[]{:S(2)}, u32[]{:S(2)}) collective-permute-start(bf16[512,512]{1,0:T(8,128)(2,1)S(1)} %get-tuple-element.62), channel_id=1, source_target_pairs={{0,48},{16,0},{32,16},{48,32},{64,112},{80,64},{96,80},{112,96},{1... | collective-permute-start | bytes 1572872 | tf_op jit(solution)/shard_map/ppermute | solution.py:382
  139.0 21.7 %collective-permute-start.27 = (bf16[512,512]{1,0:T(8,128)(2,1)S(1)}, bf16[512,512]{1,0:T(8,128)(2,1)S(1)}, u32[]{:S(2)}, u32[]{:S(2)}) collective-permute-start(bf16[512,512]{1,0:T(8,128)(2,1)S(1)} %get-tuple-element.63), channel_id=1, source_target_pairs={{0,32},{16,48},{32,0},{48,16},{64,96},{80,112},{96,64},{112,80},{1... | collective-permute-start | bytes 1572872 | tf_op jit(solution)/shard_map/ppermute | solution.py:382
  148.3 17.4 %collective-permute-start.28 = (bf16[512,512]{1,0:T(8,128)(2,1)S(1)}, bf16[512,512]{1,0:T(8,128)(2,1)S(1)}, u32[]{:S(2)}, u32[]{:S(2)}) collective-permute-start(bf16[512,512]{1,0:T(8,128)(2,1)S(1)} %get-tuple-element.64), channel_id=1, source_target_pairs={{0,16},{16,32},{32,48},{48,0},{64,80},{80,96},{96,112},{112,64},{1... | collective-permute-start | bytes 1572872 | tf_op jit(solution)/shard_map/ppermute | solution.py:382
  169.4 19.6 %collective-permute-start.29 = (bf16[512,512]{1,0:T(8,128)(2,1)S(1)}, bf16[512,512]{1,0:T(8,128)(2,1)S(1)}, u32[]{:S(2)}, u32[]{:S(2)}) collective-permute-start(bf16[512,512]{1,0:T(8,128)(2,1)S(1)} %get-tuple-element.66), channel_id=1, source_target_pairs={{0,48},{16,0},{32,16},{48,32},{64,112},{80,64},{96,80},{112,96},{1... | collective-permute-start | bytes 1572872 | tf_op jit(solution)/shard_map/ppermute | solution.py:382
  170.8 18.2 %collective-permute-start.30 = (bf16[512,512]{1,0:T(8,128)(2,1)S(1)}, bf16[512,512]{1,0:T(8,128)(2,1)S(1)}, u32[]{:S(2)}, u32[]{:S(2)}) collective-permute-start(bf16[512,512]{1,0:T(8,128)(2,1)S(1)} %get-tuple-element.67), channel_id=1, source_target_pairs={{0,16},{16,32},{32,48},{48,0},{64,80},{80,96},{96,112},{112,64},{1... | collective-permute-start | bytes 1572872 | tf_op jit(solution)/shard_map/ppermute | solution.py:382
  172.7 16.3 %collective-permute-start.31 = (bf16[512,512]{1,0:T(8,128)(2,1)S(1)}, bf16[512,512]{1,0:T(8,128)(2,1)S(1)}, u32[]{:S(2)}, u32[]{:S(2)}) collective-permute-start(bf16[512,512]{1,0:T(8,128)(2,1)S(1)} %get-tuple-element.68), channel_id=1, source_target_pairs={{0,32},{16,48},{32,0},{48,16},{64,96},{80,112},{96,64},{112,80},{1... | collective-permute-start | bytes 1572872 | tf_op jit(solution)/shard_map/ppermute | solution.py:382
  173.2 15.8 %collective-permute-start.32 = (bf16[512,512]{1,0:T(8,128)(2,1)S(1)}, bf16[512,512]{1,0:T(8,128)(2,1)S(1)}, u32[]{:S(2)}, u32[]{:S(2)}) collective-permute-start(bf16[512,512]{1,0:T(8,128)(2,1)S(1)} %get-tuple-element.70), channel_id=1, source_target_pairs={{0,192},{16,208},{32,224},{48,240},{64,0},{80,16},{96,32},{112,48}... | collective-permute-start | bytes 1572872 | tf_op jit(solution)/shard_map/ppermute | solution.py:382
  173.2 15.8 %collective-permute-start.33 = (bf16[512,512]{1,0:T(8,128)(2,1)S(1)}, bf16[512,512]{1,0:T(8,128)(2,1)S(1)}, u32[]{:S(2)}, u32[]{:S(2)}) collective-permute-start(bf16[512,512]{1,0:T(8,128)(2,1)S(1)} %get-tuple-element.71), channel_id=1, source_target_pairs={{0,64},{16,80},{32,96},{48,112},{64,128},{80,144},{96,160},{112,17... | collective-permute-start | bytes 1572872 | tf_op jit(solution)/shard_map/ppermute | solution.py:382
  (24 other events, 199.6 us)
where the time goes:
time: 202 us; the launch traced here: 201 us
  waiting for transfers between devices  106 us (52%)
  starting transfers between devices  47.8 us (24%)
  Pallas kernels  35.2 us (17%)
  local copies, waits for them, and re-layouts  11.3 us (6%)
    ppermute x26, waiting for transfers between devices, over_plane(): lax.ppermute(array, 'ep', [(y * SIDE + x, (y + by_y) % SIDE * SIDE + (x +...  75.3 us
    ppermute x26, starting transfers between devices, over_plane(): lax.ppermute(array, 'ep', [(y * SIDE + x, (y + by_y) % SIDE * SIDE + (x +...  37.5 us
    ppermute x4, waiting for transfers between devices, along_z(): lax.ppermute(array, 'tp', [(z * 2 + c, to * 2 + c) for z, c, to in pairs])  24.9 us
    pallas_call x2, Pallas kernels, expert(): pl.pallas_call(functools.partial(expert_kernel, number, [*inputs, *outs])...  16 us
    all_to_all x1, starting transfers between devices, layer(): lax.all_to_all(rows_there, 'ep', split_axis=0, concat_axis=0, tiled=True)  7.57 us
    unnamed x24, local copies, waits for them, and re-layouts  6.58 us
    pallas_call x2, Pallas kernels, pick(): pl.pallas_call(functools.partial(pick_kernel, along_y), in_specs=[SMEM] +...  6.32 us
    all_to_all x1, waiting for transfers between devices, layer(): lax.all_to_all(rows_there, 'ep', split_axis=0, concat_axis=0, tiled=True)  4.21 us
  transfers between devices with their start and end apart: 36, of which 18 were waited for; matrix products, arithmetic and copies ran while one was open for 3% of the time, Pallas kernels for 5%

commit v1 on v0

--- a/solution.py
+++ b/solution.py
@@ -414,10 +414,14 @@
     highs = [high, down, over_plane(down[:mid], 1, 0), over_plane(up[mid:], -1, 0), up]
     next2 = along_z(next1, 1, tp_count)
     picked_low = pick(True, place, rows_here, lows)
-    arrived_low = [picked_low[0]] + [over_plane(picked_low[d], d, 0) for d in range(1, SIDE)]
+    arrived_low = [picked_low[0]] + [None] * (SIDE - 1)
+    arrived_low[1], arrived_low[3] = over_plane(picked_low[1], 1, 0), over_plane(picked_low[3], 3, 0)
+    arrived_low[2] = over_plane(picked_low[2], 2, 0)
     next3 = along_z(next2, 1, tp_count)
     picked_high = pick(False, place, rows_here, highs)
-    arrived_high = [picked_high[0]] + [over_plane(picked_high[d], 0, d) for d in range(1, SIDE)]
+    arrived_high = [picked_high[0]] + [None] * (SIDE - 1)
+    arrived_high[1], arrived_high[3] = over_plane(picked_high[1], 0, 1), over_plane(picked_high[3], 0, 3)
+    arrived_high[2] = over_plane(picked_high[2], 0, 2)
     across = along_z(next2[:, : own.shape[1]], 2, tp_count)
     held = [next1, next2, next3, across]
     pieces = [both, *held, *(other_core(piece, tp_count) for piece in held)]

time: 202 us -> 202 us (level)
  no operation moved by 1% of the time
where the time goes in v1:
time: 202 us; the launch traced here: 201 us
  waiting for transfers between devices  106 us (52%)
  starting transfers between devices  47.8 us (24%)
  Pallas kernels  35.2 us (17%)
  local copies, waits for them, and re-layouts  11.3 us (6%)
    ppermute x26, waiting for transfers between devices, over_plane(): lax.ppermute(array, 'ep', [(y * SIDE + x, (y + by_y) % SIDE * SIDE + (x +...  75.3 us
    ppermute x26, starting transfers between devices, over_plane(): lax.ppermute(array, 'ep', [(y * SIDE + x, (y + by_y) % SIDE * SIDE + (x +...  37.5 us
    ppermute x4, waiting for transfers between devices, along_z(): lax.ppermute(array, 'tp', [(z * 2 + c, to * 2 + c) for z, c, to in pairs])  24.9 us
    pallas_call x2, Pallas kernels, expert(): pl.pallas_call(functools.partial(expert_kernel, number, [*inputs, *outs])...  16 us
    all_to_all x1, starting transfers between devices, layer(): lax.all_to_all(rows_there, 'ep', split_axis=0, concat_axis=0, tiled=True)  7.57 us
    unnamed x24, local copies, waits for them, and re-layouts  6.58 us
    pallas_call x2, Pallas kernels, pick(): pl.pallas_call(functools.partial(pick_kernel, along_y), in_specs=[SMEM] +...  6.32 us
    all_to_all x1, waiting for transfers between devices, layer(): lax.all_to_all(rows_there, 'ep', split_axis=0, concat_axis=0, tiled=True)  4.21 us
  transfers between devices with their start and end apart: 36, of which 18 were waited for; matrix products, arithmetic and copies ran while one was open for 3% of the time, Pallas kernels for 5%

profile of v1, /device:TPU:30, one launch (start us, length us, event | category | flops | bytes accessed | tf_op | source)
XLA Modules:
  0.0 201.4 jit_solution(3544199571778860157)
XLA Ops:
  0.0 2.6 %prepare.1 = (bf16[512,512]{1,0:T(8,128)(2,1)}, bf16[512,512]{1,0:T(8,128)(2,1)}, bf16[3,64,1024]{2,1,0:T(8,128)(2,1)}) custom-call(bf16[512,1024]{1,0:T(8,128)(2,1)} %stream_ref.1, f32[1,1024]{1,0:T(1,128)} %bitcast.7, bf16[1,64,1024]{2,1,0:T(8,128)(2,1)} %gate_ref.1, bf16[1,64,1024]{2,1,0:T(8,128)(2,1)} %up_ref.1, bf16[1,64,1024]{2,1,0:T(8,128)(2,1)} %down_ref.1), custom_call_target="tpu_custom_call" | custom-call | flops 3000000 | bytes 3145728 | tf_op jit(solution)/shard_map/prepare/pallas_call | solution.py:84
  7.7 13.9 %collective-permute-done.1.refs_1_ = bf16[3,128,1024]{2,1,0:T(8,128)(2,1)S(1)} collective-permute-done((bf16[3,128,1024]{2,1,0:T(8,128)(2,1)S(1)}, bf16[3,128,1024]{2,1,0:T(8,128)(2,1)S(1)}, u32[]{:S(2)}, u32[]{:S(2)}) %collective-permute-start.1) | collective-permute-done | bytes 786464 | tf_op jit(solution)/shard_map/ppermute | solution.py:390
  23.8 10.9 %collective-permute-done.2.refs_2_ = bf16[3,128,1024]{2,1,0:T(8,128)(2,1)S(1)} collective-permute-done((bf16[3,128,1024]{2,1,0:T(8,128)(2,1)S(1)}, bf16[3,128,1024]{2,1,0:T(8,128)(2,1)S(1)}, u32[]{:S(2)}, u32[]{:S(2)}) %collective-permute-start.2) | collective-permute-done | bytes 786464 | tf_op jit(solution)/shard_map/ppermute | solution.py:390
  43.1 7.9 %collective-permute-done.17.before_ref = bf16[512,512]{1,0:T(8,128)(2,1)} collective-permute-done((bf16[512,512]{1,0:T(8,128)(2,1)}, bf16[512,512]{1,0:T(8,128)(2,1)}, u32[]{:S(2)}, u32[]{:S(2)}) %collective-permute-start.17) | collective-permute-done | bytes 524320 | tf_op jit(solution)/shard_map/ppermute | solution.py:382
  58.0 7.6 %all-to-all-start = ((s32[16,8,128]{2,1,0:T(8,128)}), s32[16,8,128]{2,1,0:T(8,128)}, u32[]{:S(2)}, u32[]{:S(2)}) async-start(s32[16,8,128]{2,1,0:T(8,128)} %get-tuple-element.39), calls=%async_computation | async-start | bytes 131072 | tf_op jit(solution)/shard_map/all_to_all | solution.py:411
  65.7 4.2 %all-to-all-done.rows_ref = s32[16,8,128]{2,1,0:T(8,128)} async-done(((s32[16,8,128]{2,1,0:T(8,128)}), s32[16,8,128]{2,1,0:T(8,128)}, u32[]{:S(2)}, u32[]{:S(2)}) %all-to-all-start) | async-done | bytes 65568 | tf_op jit(solution)/shard_map/all_to_all | solution.py:411
  74.0 3.1 %pick_y.1 = (bf16[512,512]{1,0:T(8,128)(2,1)S(1)}, bf16[512,512]{1,0:T(8,128)(2,1)S(1)}, bf16[512,512]{1,0:T(8,128)(2,1)S(1)}, bf16[512,512]{1,0:T(8,128)(2,1)S(1)}) custom-call(s32[2]{0:T(128)S(1)} %pad_add_fusion.place_ref, s32[16,8,128]{2,1,0:T(8,128)} %all-to-all-done.rows_ref, bf16[512,512]{1,0:T(8,128)(2,1)S(1)} %copy-done.8, ...), custom_call_target="tpu_custom_call" | custom-call | flops 1073741824 | bytes 4194304 | tf_op jit(solution)/shard_map/pick_y/pallas_call | solution.py:142
  79.2 3.2 %pick_x.1 = (bf16[512,512]{1,0:T(8,128)(2,1)S(1)}, bf16[512,512]{1,0:T(8,128)(2,1)S(1)}, bf16[512,512]{1,0:T(8,128)(2,1)S(1)}, bf16[512,512]{1,0:T(8,128)(2,1)S(1)}) custom-call(s32[2]{0:T(128)S(1)} %pad_add_fusion.place_ref, s32[16,8,128]{2,1,0:T(8,128)} %all-to-all-done.rows_ref, bf16[512,512]{1,0:T(8,128)(2,1)S(1)} %copy-done.7, ...), custom_call_target="tpu_custom_call" | custom-call | flops 1073741824 | bytes 4194304 | tf_op jit(solution)/shard_map/pick_x/pallas_call | solution.py:142
  82.5 7.6 %collective-permute-done.13.refs_2_.refs_0_ = bf16[512,512]{1,0:T(8,128)(2,1)S(1)} collective-permute-done((bf16[512,512]{1,0:T(8,128)(2,1)S(1)}, bf16[512,512]{1,0:T(8,128)(2,1)S(1)}, u32[]{:S(2)}, u32[]{:S(2)}) %collective-permute-start.13) | collective-permute-done | bytes 524320 | tf_op jit(solution)/shard_map/ppermute | solution.py:382
  94.1 3.9 %collective-permute-start.21 = (bf16[512,512]{1,0:T(8,128)(2,1)S(1)}, bf16[512,512]{1,0:T(8,128)(2,1)S(1)}, u32[]{:S(2)}, u32[]{:S(2)}) collective-permute-start(bf16[512,512]{1,0:T(8,128)(2,1)S(1)} %get-tuple-element.53), channel_id=1, source_target_pairs={{0,128},{16,144},{32,160},{48,176},{64,192},{80,208},{96,224},{112... | collective-permute-start | bytes 1572872 | tf_op jit(solution)/shard_map/ppermute | solution.py:382
  101.0 4.2 %collective-permute-done.14.refs_3_.refs_2_ = bf16[512,512]{1,0:T(8,128)(2,1)S(1)} collective-permute-done((bf16[512,512]{1,0:T(8,128)(2,1)S(1)}, bf16[512,512]{1,0:T(8,128)(2,1)S(1)}, u32[]{:S(2)}, u32[]{:S(2)}) %collective-permute-start.14) | collective-permute-done | bytes 524320 | tf_op jit(solution)/shard_map/ppermute | solution.py:382
  106.6 8.0 %collective-permute-done.20.refs_5_ = bf16[512,512]{1,0:T(8,128)(2,1)S(1)} collective-permute-done((bf16[512,512]{1,0:T(8,128)(2,1)S(1)}, bf16[512,512]{1,0:T(8,128)(2,1)S(1)}, u32[]{:S(2)}, u32[]{:S(2)}) %collective-permute-start.20) | collective-permute-done | bytes 524320 | tf_op jit(solution)/shard_map/ppermute | solution.py:382
  116.0 8.0 %shard_map.74 = (bf16[512,512]{1,0:T(8,128)(2,1)S(1)}, bf16[512,512]{1,0:T(8,128)(2,1)S(1)}, bf16[1024,512]{1,0:T(8,128)(2,1)S(1)}, bf16[1024,512]{1,0:T(8,128)(2,1)S(1)}) custom-call(s32[2]{0:T(128)S(1)} %pad_add_fusion.place_ref, f32[16,128]{1,0:T(8,128)S(1)} %copy-done.11, bf16[1024,1024]{1,0:T(8,128)(2,1)S(1)} %get-tuple-element.42.gate_ref, ...), custom_call_target="tpu_custom_call" | custom-call | flops 6442450944 | bytes 4194304 | tf_op jit(solution)/shard_map/pallas_call | solution.py:294
  124.0 8.0 %shard_map.75 = (bf16[512,512]{1,0:T(8,128)(2,1)S(1)}, bf16[512,512]{1,0:T(8,128)(2,1)S(1)}, bf16[512,512]{1,0:T(8,128)(2,1)S(1)}, bf16[512,512]{1,0:T(8,128)(2,...) custom-call(s32[2]{0:T(128)S(1)} %pad_add_fusion.place_ref, f32[16,128]{1,0:T(8,128)S(1)} %copy-done.11, ...), custom_call_target="tpu_custom_call" | custom-call | flops 6442450944 | bytes 4194304 | tf_op jit(solution)/shard_map/pallas_call | solution.py:294
  132.4 3.0 %collective-permute-start.24 = (bf16[512,512]{1,0:T(8,128)(2,1)S(1)}, bf16[512,512]{1,0:T(8,128)(2,1)S(1)}, u32[]{:S(2)}, u32[]{:S(2)}) collective-permute-start(bf16[512,512]{1,0:T(8,128)(2,1)S(1)} %get-tuple-element.59), channel_id=1, source_target_pairs={{0,128},{16,144},{32,160},{48,176},{64,192},{80,208},{96,224},{112... | collective-permute-start | bytes 1572872 | tf_op jit(solution)/shard_map/ppermute | solution.py:382
  139.0 3.2 %collective-permute-start.27 = (bf16[512,512]{1,0:T(8,128)(2,1)S(1)}, bf16[512,512]{1,0:T(8,128)(2,1)S(1)}, u32[]{:S(2)}, u32[]{:S(2)}) collective-permute-start(bf16[512,512]{1,0:T(8,128)(2,1)S(1)} %get-tuple-element.63), channel_id=1, source_target_pairs={{0,32},{16,48},{32,0},{48,16},{64,96},{80,112},{96,64},{112,80},{1... | collective-permute-start | bytes 1572872 | tf_op jit(solution)/shard_map/ppermute | solution.py:382
  142.2 6.1 %collective-permute-done.23.refs_1_ = bf16[512,512]{1,0:T(8,128)(2,1)S(1)} collective-permute-done((bf16[512,512]{1,0:T(8,128)(2,1)S(1)}, bf16[512,512]{1,0:T(8,128)(2,1)S(1)}, u32[]{:S(2)}, u32[]{:S(2)}) %collective-permute-start.23) | collective-permute-done | bytes 524320 | tf_op jit(solution)/shard_map/ppermute | solution.py:382
  150.2 5.6 %collective-permute-done.24.refs_2_ = bf16[512,512]{1,0:T(8,128)(2,1)S(1)} collective-permute-done((bf16[512,512]{1,0:T(8,128)(2,1)S(1)}, bf16[512,512]{1,0:T(8,128)(2,1)S(1)}, u32[]{:S(2)}, u32[]{:S(2)}) %collective-permute-start.24) | collective-permute-done | bytes 524320 | tf_op jit(solution)/shard_map/ppermute | solution.py:382
  156.4 4.3 %collective-permute-done.27.refs_6_ = bf16[512,512]{1,0:T(8,128)(2,1)S(1)} collective-permute-done((bf16[512,512]{1,0:T(8,128)(2,1)S(1)}, bf16[512,512]{1,0:T(8,128)(2,1)S(1)}, u32[]{:S(2)}, u32[]{:S(2)}) %collective-permute-start.27) | collective-permute-done | bytes 524320 | tf_op jit(solution)/shard_map/ppermute | solution.py:382
  160.7 5.0 %collective-permute-done.28.refs_7_ = bf16[512,512]{1,0:T(8,128)(2,1)S(1)} collective-permute-done((bf16[512,512]{1,0:T(8,128)(2,1)S(1)}, bf16[512,512]{1,0:T(8,128)(2,1)S(1)}, u32[]{:S(2)}, u32[]{:S(2)}) %collective-permute-start.28) | collective-permute-done | bytes 524320 | tf_op jit(solution)/shard_map/ppermute | solution.py:382
  165.7 3.7 %relay.1 = (bf16[512,512]{1,0:T(8,128)(2,1)S(1)}, bf16[512,512]{1,0:T(8,128)(2,1)S(1)}, bf16[512,512]{1,0:T(8,128)(2,1)S(1)}, bf16[512,512]{1,0:T(8,128)(2,1)S(1...) custom-call(s32[2]{0:T(128)S(1)} %pad_add_fusion.place_ref, ...), custom_call_target="tpu_custom_call" | custom-call | flops 2147483648 | bytes 8388608 | tf_op jit(solution)/shard_map/relay/pallas_call | solution.py:343
  173.2 3.2 %collective-permute-start.33 = (bf16[512,512]{1,0:T(8,128)(2,1)S(1)}, bf16[512,512]{1,0:T(8,128)(2,1)S(1)}, u32[]{:S(2)}, u32[]{:S(2)}) collective-permute-start(bf16[512,512]{1,0:T(8,128)(2,1)S(1)} %get-tuple-element.71), channel_id=1, source_target_pairs={{0,64},{16,80},{32,96},{48,112},{64,128},{80,144},{96,160},{112,17... | collective-permute-start | bytes 1572872 | tf_op jit(solution)/shard_map/ppermute | solution.py:382
  176.4 12.6 %collective-permute-done.29.refs_1_ = bf16[512,512]{1,0:T(8,128)(2,1)S(1)} collective-permute-done((bf16[512,512]{1,0:T(8,128)(2,1)S(1)}, bf16[512,512]{1,0:T(8,128)(2,1)S(1)}, u32[]{:S(2)}, u32[]{:S(2)}) %collective-permute-start.29) | collective-permute-done | bytes 524320 | tf_op jit(solution)/shard_map/ppermute | solution.py:382
  189.0 10.7 %collective-permute-done.34.refs_7_ = bf16[512,512]{1,0:T(8,128)(2,1)S(1)} collective-permute-done((bf16[512,512]{1,0:T(8,128)(2,1)S(1)}, bf16[512,512]{1,0:T(8,128)(2,1)S(1)}, u32[]{:S(2)}, u32[]{:S(2)}) %collective-permute-start.34) | collective-permute-done | bytes 524320 | tf_op jit(solution)/shard_map/ppermute | solution.py:382
  (89 shorter events, 50.9 us)
Async XLA Ops:
  5.7 15.9 %collective-permute-start.1 = (bf16[3,128,1024]{2,1,0:T(8,128)(2,1)S(1)}, bf16[3,128,1024]{2,1,0:T(8,128)(2,1)S(1)}, u32[]{:S(2)}, u32[]{:S(2)}) collective-permute-start(bf16[3,128,1024]{2,1,0:T(8,128)(2,1)S(1)} %shard_map.73.refs_0_), channel_id=1, source_target_pairs={{0,2},{1,15},{2,4},{3,1},{4,6},{5,3},{6,8},{7,5},{8,10},{9,7},{10,... | collective-permute-start | bytes 2359304 | tf_op jit(solution)/shard_map/ppermute | solution.py:390
  22.1 16.0 %collective-permute-start.11 = (bf16[512,512]{1,0:T(8,128)(2,1)}, bf16[512,512]{1,0:T(8,128)(2,1)S(1)}, u32[]{:S(2)}, u32[]{:S(2)}) collective-permute-start(bf16[512,512]{1,0:T(8,128)(2,1)} %get-tuple-element.45.own_ref), channel_id=1, source_target_pairs={{0,48},{16,0},{32,16},{48,32},{64,112},{80,64},{96,80},{112,96},{1... | collective-permute-start | bytes 1572872 | tf_op jit(solution)/shard_map/ppermute | solution.py:382
  34.8 20.0 %collective-permute-start.3 = (bf16[3,128,1024]{2,1,0:T(8,128)(2,1)S(1)}, bf16[3,128,1024]{2,1,0:T(8,128)(2,1)S(1)}, u32[]{:S(2)}, u32[]{:S(2)}) collective-permute-start(bf16[3,128,1024]{2,1,0:T(8,128)(2,1)S(1)} %collective-permute-done.2.refs_2_), channel_id=1, source_target_pairs={{0,2},{1,15},{2,4},{3,1},{4,6},{5,3},{6,8},{7,5},{8,10},{9,7},{10,... | collective-permute-start | bytes 2359304 | tf_op jit(solution)/shard_map/ppermute | solution.py:390
  34.8 16.2 %collective-permute-start.17 = (bf16[512,512]{1,0:T(8,128)(2,1)}, bf16[512,512]{1,0:T(8,128)(2,1)}, u32[]{:S(2)}, u32[]{:S(2)}) collective-permute-start(bf16[512,512]{1,0:T(8,128)(2,1)} %get-tuple-element.49.own_ref), channel_id=1, source_target_pairs={{0,192},{16,208},{32,224},{48,240},{64,0},{80,16},{96,32},{112,48}... | collective-permute-start | bytes 1572872 | tf_op jit(solution)/shard_map/ppermute | solution.py:382
  36.4 17.1 %collective-permute-start.10 = (bf16[256,512]{1,0:T(8,128)(2,1)}, bf16[256,512]{1,0:T(8,128)(2,1)S(1)}, u32[]{:S(2)}, u32[]{:S(2)}) collective-permute-start(bf16[256,512]{1,0:T(8,128)(2,1)} %slice.21), channel_id=1, source_target_pairs={{0,16},{16,32},{32,48},{48,0},{64,80},{80,96},{96,112},{112,64},{1... | collective-permute-start | bytes 786440 | tf_op jit(solution)/shard_map/ppermute | solution.py:382
  52.7 24.4 %collective-permute-start.18 = (bf16[256,512]{1,0:T(8,128)(2,1)}, bf16[256,512]{1,0:T(8,128)(2,1)}, u32[]{:S(2)}, u32[]{:S(2)}) collective-permute-start(bf16[256,512]{1,0:T(8,128)(2,1)} %slice.24), channel_id=1, source_target_pairs={{0,192},{16,208},{32,224},{48,240},{64,0},{80,16},{96,32},{112,48}... | collective-permute-start | bytes 786440 | tf_op jit(solution)/shard_map/ppermute | solution.py:382
  54.2 36.7 %collective-permute-start.5 = (bf16[3,128,1024]{2,1,0:T(8,128)(2,1)S(1)}, bf16[3,128,1024]{2,1,0:T(8,128)(2,1)}, u32[]{:S(2)}, u32[]{:S(2)}) collective-permute-start(bf16[3,128,1024]{2,1,0:T(8,128)(2,1)S(1)} %collective-permute-done.1.refs_1_), channel_id=1, source_target_pairs={{0,1},{1,0},{2,3},{3,2},{4,5},{5,4},{6,7},{7,6},{8,9},{9,8},{10,11... | collective-permute-start | bytes 2359304 | tf_op jit(solution)/shard_map/ppermute | solution.py:394
  54.3 24.9 %collective-permute-start.4 = (bf16[3,64,1024]{2,1,0:T(8,128)(2,1)}, bf16[3,64,1024]{2,1,0:T(8,128)(2,1)S(1)}, u32[]{:S(2)}, u32[]{:S(2)}) collective-permute-start(bf16[3,64,1024]{2,1,0:T(8,128)(2,1)} %slice.20), channel_id=1, source_target_pairs={{0,4},{1,13},{2,6},{3,15},{4,8},{5,1},{6,10},{7,3},{8,12},{9,5},{1... | collective-permute-start | bytes 1179656 | tf_op jit(solution)/shard_map/ppermute | solution.py:390
  54.3 37.3 %collective-permute-start.6 = (bf16[3,128,1024]{2,1,0:T(8,128)(2,1)S(1)}, bf16[3,128,1024]{2,1,0:T(8,128)(2,1)}, u32[]{:S(2)}, u32[]{:S(2)}) collective-permute-start(bf16[3,128,1024]{2,1,0:T(8,128)(2,1)S(1)} %collective-permute-done.2.refs_2_), channel_id=1, source_target_pairs={{0,1},{1,0},{2,3},{3,2},{4,5},{5,4},{6,7},{7,6},{8,9},{9,8},{10,11... | collective-permute-start | bytes 2359304 | tf_op jit(solution)/shard_map/ppermute | solution.py:394
  54.8 43.3 %collective-permute-start.7 = (bf16[3,128,1024]{2,1,0:T(8,128)(2,1)S(1)}, bf16[3,128,1024]{2,1,0:T(8,128)(2,1)}, u32[]{:S(2)}, u32[]{:S(2)}) collective-permute-start(bf16[3,128,1024]{2,1,0:T(8,128)(2,1)S(1)} %collective-permute-done.3.refs_3_), channel_id=1, source_target_pairs={{0,1},{1,0},{2,3},{3,2},{4,5},{5,4},{6,7},{7,6},{8,9},{9,8},{10,11... | collective-permute-start | bytes 2359304 | tf_op jit(solution)/shard_map/ppermute | solution.py:394
  91.6 23.0 %collective-permute-start.20 = (bf16[512,512]{1,0:T(8,128)(2,1)S(1)}, bf16[512,512]{1,0:T(8,128)(2,1)S(1)}, u32[]{:S(2)}, u32[]{:S(2)}) collective-permute-start(bf16[512,512]{1,0:T(8,128)(2,1)S(1)} %get-tuple-element.52), channel_id=1, source_target_pairs={{0,16},{16,32},{32,48},{48,0},{64,80},{80,96},{96,112},{112,64},{1... | collective-permute-start | bytes 1572872 | tf_op jit(solution)/shard_map/ppermute | solution.py:382
  94.1 21.9 %collective-permute-start.21 = (bf16[512,512]{1,0:T(8,128)(2,1)S(1)}, bf16[512,512]{1,0:T(8,128)(2,1)S(1)}, u32[]{:S(2)}, u32[]{:S(2)}) collective-permute-start(bf16[512,512]{1,0:T(8,128)(2,1)S(1)} %get-tuple-element.53), channel_id=1, source_target_pairs={{0,128},{16,144},{32,160},{48,176},{64,192},{80,208},{96,224},{112... | collective-permute-start | bytes 1572872 | tf_op jit(solution)/shard_map/ppermute | solution.py:382
  98.0 18.0 %collective-permute-start.22 = (bf16[512,512]{1,0:T(8,128)(2,1)S(1)}, bf16[512,512]{1,0:T(8,128)(2,1)S(1)}, u32[]{:S(2)}, u32[]{:S(2)}) collective-permute-start(bf16[512,512]{1,0:T(8,128)(2,1)S(1)} %get-tuple-element.54), channel_id=1, source_target_pairs={{0,32},{16,48},{32,0},{48,16},{64,96},{80,112},{96,64},{112,80},{1... | collective-permute-start | bytes 1572872 | tf_op jit(solution)/shard_map/ppermute | solution.py:382
  132.1 16.2 %collective-permute-start.23 = (bf16[512,512]{1,0:T(8,128)(2,1)S(1)}, bf16[512,512]{1,0:T(8,128)(2,1)S(1)}, u32[]{:S(2)}, u32[]{:S(2)}) collective-permute-start(bf16[512,512]{1,0:T(8,128)(2,1)S(1)} %get-tuple-element.58), channel_id=1, source_target_pairs={{0,192},{16,208},{32,224},{48,240},{64,0},{80,16},{96,32},{112,48}... | collective-permute-start | bytes 1572872 | tf_op jit(solution)/shard_map/ppermute | solution.py:382
  132.4 23.3 %collective-permute-start.24 = (bf16[512,512]{1,0:T(8,128)(2,1)S(1)}, bf16[512,512]{1,0:T(8,128)(2,1)S(1)}, u32[]{:S(2)}, u32[]{:S(2)}) collective-permute-start(bf16[512,512]{1,0:T(8,128)(2,1)S(1)} %get-tuple-element.59), channel_id=1, source_target_pairs={{0,128},{16,144},{32,160},{48,176},{64,192},{80,208},{96,224},{112... | collective-permute-start | bytes 1572872 | tf_op jit(solution)/shard_map/ppermute | solution.py:382
  135.5 20.9 %collective-permute-start.25 = (bf16[512,512]{1,0:T(8,128)(2,1)S(1)}, bf16[512,512]{1,0:T(8,128)(2,1)S(1)}, u32[]{:S(2)}, u32[]{:S(2)}) collective-permute-start(bf16[512,512]{1,0:T(8,128)(2,1)S(1)} %get-tuple-element.60), channel_id=1, source_target_pairs={{0,64},{16,80},{32,96},{48,112},{64,128},{80,144},{96,160},{112,17... | collective-permute-start | bytes 1572872 | tf_op jit(solution)/shard_map/ppermute | solution.py:382
  137.8 18.6 %collective-permute-start.26 = (bf16[512,512]{1,0:T(8,128)(2,1)S(1)}, bf16[512,512]{1,0:T(8,128)(2,1)S(1)}, u32[]{:S(2)}, u32[]{:S(2)}) collective-permute-start(bf16[512,512]{1,0:T(8,128)(2,1)S(1)} %get-tuple-element.62), channel_id=1, source_target_pairs={{0,48},{16,0},{32,16},{48,32},{64,112},{80,64},{96,80},{112,96},{1... | collective-permute-start | bytes 1572872 | tf_op jit(solution)/shard_map/ppermute | solution.py:382
  139.0 21.7 %collective-permute-start.27 = (bf16[512,512]{1,0:T(8,128)(2,1)S(1)}, bf16[512,512]{1,0:T(8,128)(2,1)S(1)}, u32[]{:S(2)}, u32[]{:S(2)}) collective-permute-start(bf16[512,512]{1,0:T(8,128)(2,1)S(1)} %get-tuple-element.63), channel_id=1, source_target_pairs={{0,32},{16,48},{32,0},{48,16},{64,96},{80,112},{96,64},{112,80},{1... | collective-permute-start | bytes 1572872 | tf_op jit(solution)/shard_map/ppermute | solution.py:382
  148.3 17.4 %collective-permute-start.28 = (bf16[512,512]{1,0:T(8,128)(2,1)S(1)}, bf16[512,512]{1,0:T(8,128)(2,1)S(1)}, u32[]{:S(2)}, u32[]{:S(2)}) collective-permute-start(bf16[512,512]{1,0:T(8,128)(2,1)S(1)} %get-tuple-element.64), channel_id=1, source_target_pairs={{0,16},{16,32},{32,48},{48,0},{64,80},{80,96},{96,112},{112,64},{1... | collective-permute-start | bytes 1572872 | tf_op jit(solution)/shard_map/ppermute | solution.py:382
  169.4 19.6 %collective-permute-start.29 = (bf16[512,512]{1,0:T(8,128)(2,1)S(1)}, bf16[512,512]{1,0:T(8,128)(2,1)S(1)}, u32[]{:S(2)}, u32[]{:S(2)}) collective-permute-start(bf16[512,512]{1,0:T(8,128)(2,1)S(1)} %get-tuple-element.66), channel_id=1, source_target_pairs={{0,48},{16,0},{32,16},{48,32},{64,112},{80,64},{96,80},{112,96},{1... | collective-permute-start | bytes 1572872 | tf_op jit(solution)/shard_map/ppermute | solution.py:382
  170.8 18.2 %collective-permute-start.30 = (bf16[512,512]{1,0:T(8,128)(2,1)S(1)}, bf16[512,512]{1,0:T(8,128)(2,1)S(1)}, u32[]{:S(2)}, u32[]{:S(2)}) collective-permute-start(bf16[512,512]{1,0:T(8,128)(2,1)S(1)} %get-tuple-element.67), channel_id=1, source_target_pairs={{0,16},{16,32},{32,48},{48,0},{64,80},{80,96},{96,112},{112,64},{1... | collective-permute-start | bytes 1572872 | tf_op jit(solution)/shard_map/ppermute | solution.py:382
  172.7 16.3 %collective-permute-start.31 = (bf16[512,512]{1,0:T(8,128)(2,1)S(1)}, bf16[512,512]{1,0:T(8,128)(2,1)S(1)}, u32[]{:S(2)}, u32[]{:S(2)}) collective-permute-start(bf16[512,512]{1,0:T(8,128)(2,1)S(1)} %get-tuple-element.68), channel_id=1, source_target_pairs={{0,32},{16,48},{32,0},{48,16},{64,96},{80,112},{96,64},{112,80},{1... | collective-permute-start | bytes 1572872 | tf_op jit(solution)/shard_map/ppermute | solution.py:382
  173.2 15.8 %collective-permute-start.32 = (bf16[512,512]{1,0:T(8,128)(2,1)S(1)}, bf16[512,512]{1,0:T(8,128)(2,1)S(1)}, u32[]{:S(2)}, u32[]{:S(2)}) collective-permute-start(bf16[512,512]{1,0:T(8,128)(2,1)S(1)} %get-tuple-element.70), channel_id=1, source_target_pairs={{0,192},{16,208},{32,224},{48,240},{64,0},{80,16},{96,32},{112,48}... | collective-permute-start | bytes 1572872 | tf_op jit(solution)/shard_map/ppermute | solution.py:382
  173.2 15.8 %collective-permute-start.33 = (bf16[512,512]{1,0:T(8,128)(2,1)S(1)}, bf16[512,512]{1,0:T(8,128)(2,1)S(1)}, u32[]{:S(2)}, u32[]{:S(2)}) collective-permute-start(bf16[512,512]{1,0:T(8,128)(2,1)S(1)} %get-tuple-element.71), channel_id=1, source_target_pairs={{0,64},{16,80},{32,96},{48,112},{64,128},{80,144},{96,160},{112,17... | collective-permute-start | bytes 1572872 | tf_op jit(solution)/shard_map/ppermute | solution.py:382
  (24 other events, 199.6 us)

commit v2 on v1

--- a/solution.py
+++ b/solution.py
@@ -205,12 +205,14 @@
 
 
 STEPS = (
-    ((2, 0), (2, 1), (2, 2), (2, 3), (0, 2), (1, 2), (3, 2), (1, 1)),
-    ((1, 0), (1, 3), (0, 1), (3, 1), (3, 0), (3, 3), (0, 3), (0, 0)),
+    ((0, 0), (1, 0), (2, 0), (3, 0)),
+    ((2, 1), (2, 2), (2, 3), (0, 2), (1, 2), (3, 2)),
+    ((0, 1), (1, 1), (3, 1), (0, 3), (1, 3), (3, 3)),
 )
 FINISHED = (
+    (("high", 0),),
     (("low", 2), ("high", 2)),
-    (("low", 1), ("high", 1), ("low", 3), ("high", 3), ("low", 0), ("high", 0)),
+    (("low", 1), ("high", 1), ("low", 3), ("high", 3), ("low", 0)),
 )
 
 
@@ -233,7 +235,7 @@
         columns_ref[at, :] = jnp.broadcast_to(line, (slots, slots)).T
     last = (((1,), (1,)), ((), ()))
     units = gate_ref.shape[0]
-    width, rows = units // 4, SIDE * slots
+    width, rows = units // 4, 2 * slots
 
     def work(i, carry):
         at = pl.ds(pl.multiple_of(i * rows, rows), rows)
@@ -247,7 +249,7 @@
         result_ref[at, :] = (result * columns_ref[at, :][:, :1]).astype(jnp.bfloat16)
         return carry
 
-    lax.fori_loop(0, len(blocks) // SIDE, work, 0)
+    lax.fori_loop(0, len(blocks) // 2, work, 0)
 
     def part(block, which):
         if block in blocks:

time: 202 us -> 197 us (0.975)
  the two profiles are of different devices: /device:TPU:30 before, /device:TPU:32 now
where the time goes in v2:
time: 197 us
  waiting for transfers between devices  101 us (51%)
  starting transfers between devices  48.2 us (24%)
  Pallas kernels  36.1 us (18%)
  local copies, waits for them, and re-layouts  10.5 us (5%)
    ppermute x26, waiting for transfers between devices, over_plane(): lax.ppermute(array, 'ep', [(y * SIDE + x, (y + by_y) % SIDE * SIDE + (x +...  66.4 us
    ppermute x26, starting transfers between devices, over_plane(): lax.ppermute(array, 'ep', [(y * SIDE + x, (y + by_y) % SIDE * SIDE + (x +...  36.2 us
    ppermute x4, waiting for transfers between devices, along_z(): lax.ppermute(array, 'tp', [(z * 2 + c, to * 2 + c) for z, c, to in pairs])  25.4 us
    pallas_call x3, Pallas kernels, expert(): pl.pallas_call(functools.partial(expert_kernel, number, [*inputs, *outs])...  17.6 us
    ppermute x4, starting transfers between devices, along_z(): lax.ppermute(array, 'tp', [(z * 2 + c, to * 2 + c) for z, c, to in pairs])  8.31 us
    all_to_all x1, waiting for transfers between devices, layer(): lax.all_to_all(rows_there, 'ep', split_axis=0, concat_axis=0, tiled=True)  7.51 us
    pallas_call x2, Pallas kernels, pick(): pl.pallas_call(functools.partial(pick_kernel, along_y), in_specs=[SMEM] +...  6.38 us
    unnamed x16, local copies, waits for them, and re-layouts  5.72 us
  transfers between devices with their start and end apart: 36, of which 15 were waited for; matrix products, arithmetic and copies ran while one was open for 3% of the time, Pallas kernels for 8%

profile of v2, /device:TPU:32, one launch (start us, length us, event | category | flops | bytes accessed | tf_op | source)
XLA Modules:
  0.0 196.9 jit_solution(8243340165017444576)
XLA Ops:
  7.7 10.1 %collective-permute-done.1.refs_1_ = bf16[3,128,1024]{2,1,0:T(8,128)(2,1)S(1)} collective-permute-done((bf16[3,128,1024]{2,1,0:T(8,128)(2,1)S(1)}, bf16[3,128,1024]{2,1,0:T(8,128)(2,1)S(1)}, u32[]{:S(2)}, u32[]{:S(2)}) %collective-permute-start.1) | collective-permute-done | bytes 786464 | tf_op jit(solution)/shard_map/ppermute | solution.py:392
  26.1 5.5 %collective-permute-done.2.refs_2_ = bf16[3,128,1024]{2,1,0:T(8,128)(2,1)S(1)} collective-permute-done((bf16[3,128,1024]{2,1,0:T(8,128)(2,1)S(1)}, bf16[3,128,1024]{2,1,0:T(8,128)(2,1)S(1)}, u32[]{:S(2)}, u32[]{:S(2)}) %collective-permute-start.2) | collective-permute-done | bytes 786464 | tf_op jit(solution)/shard_map/ppermute | solution.py:392
  31.7 3.7 %collective-permute-done.9.after_ref = bf16[512,512]{1,0:T(8,128)(2,1)S(1)} collective-permute-done((bf16[512,512]{1,0:T(8,128)(2,1)}, bf16[512,512]{1,0:T(8,128)(2,1)S(1)}, u32[]{:S(2)}, u32[]{:S(2)}) %collective-permute-start.9) | collective-permute-done | bytes 524320 | tf_op jit(solution)/shard_map/ppermute | solution.py:384
  38.8 3.0 %collective-permute-start.12 = (bf16[256,512]{1,0:T(8,128)(2,1)}, bf16[256,512]{1,0:T(8,128)(2,1)}, u32[]{:S(2)}, u32[]{:S(2)}) collective-permute-start(bf16[256,512]{1,0:T(8,128)(2,1)} %slice.22), channel_id=1, source_target_pairs={{0,48},{16,0},{32,16},{48,32},{64,112},{80,64},{96,80},{112,96},{1... | collective-permute-start | bytes 786440 | tf_op jit(solution)/shard_map/ppermute | solution.py:384
  51.4 3.5 %all-to-all-start = ((s32[16,8,128]{2,1,0:T(8,128)}), s32[16,8,128]{2,1,0:T(8,128)S(1)}, u32[]{:S(2)}, u32[]{:S(2)}) async-start(s32[16,8,128]{2,1,0:T(8,128)} %get-tuple-element.40), calls=%async_computation | async-start | bytes 131072 | tf_op jit(solution)/shard_map/all_to_all | solution.py:413
  55.0 7.5 %all-to-all-done.rows_ref = s32[16,8,128]{2,1,0:T(8,128)S(1)} async-done(((s32[16,8,128]{2,1,0:T(8,128)}), s32[16,8,128]{2,1,0:T(8,128)S(1)}, u32[]{:S(2)}, u32[]{:S(2)}) %all-to-all-start) | async-done | bytes 65568 | tf_op jit(solution)/shard_map/all_to_all | solution.py:413
  65.7 3.1 %pick_y.1 = (bf16[512,512]{1,0:T(8,128)(2,1)S(1)}, bf16[512,512]{1,0:T(8,128)(2,1)S(1)}, bf16[512,512]{1,0:T(8,128)(2,1)S(1)}, bf16[512,512]{1,0:T(8,128)(2,1)S(1)}) custom-call(s32[2]{0:T(128)S(1)} %pad_add_fusion.place_ref, s32[16,8,128]{2,1,0:T(8,128)S(1)} %all-to-all-done.rows_ref, bf16[512,512]{1,0:T(8,128)(2,1)S(1)} %copy-done.6, ...), custom_call_target="tpu_custom_call" | custom-call | flops 1073741824 | bytes 4194304 | tf_op jit(solution)/shard_map/pick_y/pallas_call | solution.py:142
  69.7 4.3 %collective-permute-start.4 = (bf16[3,64,1024]{2,1,0:T(8,128)(2,1)S(1)}, bf16[3,64,1024]{2,1,0:T(8,128)(2,1)S(1)}, u32[]{:S(2)}, u32[]{:S(2)}) collective-permute-start(bf16[3,64,1024]{2,1,0:T(8,128)(2,1)S(1)} %slice.20), channel_id=1, source_target_pairs={{0,4},{1,13},{2,6},{3,15},{4,8},{5,1},{6,10},{7,3},{8,12},{9,5},{1... | collective-permute-start | bytes 1179656 | tf_op jit(solution)/shard_map/ppermute | solution.py:392
  74.1 9.9 %collective-permute-done.4.refs_4_ = bf16[3,64,1024]{2,1,0:T(8,128)(2,1)S(1)} collective-permute-done((bf16[3,64,1024]{2,1,0:T(8,128)(2,1)S(1)}, bf16[3,64,1024]{2,1,0:T(8,128)(2,1)S(1)}, u32[]{:S(2)}, u32[]{:S(2)}) %collective-permute-start.4) | collective-permute-done | bytes 393248 | tf_op jit(solution)/shard_map/ppermute | solution.py:392
  86.6 3.3 %pick_x.1 = (bf16[512,512]{1,0:T(8,128)(2,1)S(1)}, bf16[512,512]{1,0:T(8,128)(2,1)S(1)}, bf16[512,512]{1,0:T(8,128)(2,1)S(1)}, bf16[512,512]{1,0:T(8,128)(2,1)S(1)}) custom-call(s32[2]{0:T(128)S(1)} %pad_add_fusion.place_ref, s32[16,8,128]{2,1,0:T(8,128)S(1)} %all-to-all-done.rows_ref, bf16[512,512]{1,0:T(8,128)(2,1)S(1)} %copy-done.5, ...), custom_call_target="tpu_custom_call" | custom-call | flops 1073741824 | bytes 4194304 | tf_op jit(solution)/shard_map/pick_x/pallas_call | solution.py:142
  95.0 14.7 %collective-permute-done.14.refs_3_.refs_2_ = bf16[512,512]{1,0:T(8,128)(2,1)S(1)} collective-permute-done((bf16[512,512]{1,0:T(8,128)(2,1)S(1)}, bf16[512,512]{1,0:T(8,128)(2,1)S(1)}, u32[]{:S(2)}, u32[]{:S(2)}) %collective-permute-start.14) | collective-permute-done | bytes 524320 | tf_op jit(solution)/shard_map/ppermute | solution.py:384
  109.7 4.5 %shard_map.74 = (bf16[512,512]{1,0:T(8,128)(2,1)S(1)}, bf16[512,512]{1,0:T(8,128)(2,1)S(1)}) custom-call(s32[2]{0:T(128)S(1)} %pad_add_fusion.place_ref, f32[16,128]{1,0:T(8,128)S(1)} %copy-done.7, bf16[1024,1024]{1,0:T(8,128)(2,1)S(1)} %get-tuple-element.43.gate_ref, bf16[1024,1024]{1,0:T(8,128)(2,1)S(1)} %get-tuple-element.44.up_ref, ...), custom_call_target="tpu_custom_call" | custom-call | flops 3221225472 | bytes 2097152 | tf_op jit(solution)/shard_map/pallas_call | solution.py:296
  116.5 6.5 %shard_map.75 = (bf16[512,512]{1,0:T(8,128)(2,1)S(1)}, bf16[512,512]{1,0:T(8,128)(2,1)S(1)}, bf16[768,512]{1,0:T(8,128)(2,1)S(1)}, bf16[768,512]{1,0:T(8,128)(2,1)S(1)}) custom-call(s32[2]{0:T(128)S(1)} %pad_add_fusion.place_ref, f32[16,128]{1,0:T(8,128)S(1)} %copy-done.7, bf16[1024,1024]{1,0:T(8,128)(2,1)S(1)} %get-tuple-element.43.gate_ref, ...), custom_call_target="tpu_custom_call" | custom-call | flops 4831838208 | bytes 3145728 | tf_op jit(solution)/shard_map/pallas_call | solution.py:296
  123.1 6.5 %shard_map.76 = (bf16[512,512]{1,0:T(8,128)(2,1)S(1)}, bf16[512,512]{1,0:T(8,128)(2,1)S(1)}, bf16[512,512]{1,0:T(8,128)(2,1)S(1)}, bf16[512,512]{1,0:T(8,128)(2,1)S(1)}, bf16[512,512]{1,0:T(8,128)(2,1)S(1)}) custom-call(s32[2]{0:T(128)S(1)} %pad_add_fusion.place_ref, f32[16,128]{1,0:T(8,128)S(1)} %copy-done.7, ...), custom_call_target="tpu_custom_call" | custom-call | flops 4831838208 | bytes 3145728 | tf_op jit(solution)/shard_map/pallas_call | solution.py:296
  134.3 3.0 %collective-permute-start.26 = (bf16[512,512]{1,0:T(8,128)(2,1)S(1)}, bf16[512,512]{1,0:T(8,128)(2,1)S(1)}, u32[]{:S(2)}, u32[]{:S(2)}) collective-permute-start(bf16[512,512]{1,0:T(8,128)(2,1)S(1)} %get-tuple-element.64), channel_id=1, source_target_pairs={{0,48},{16,0},{32,16},{48,32},{64,112},{80,64},{96,80},{112,96},{1... | collective-permute-start | bytes 1572872 | tf_op jit(solution)/shard_map/ppermute | solution.py:384
  137.3 16.1 %collective-permute-done.23.refs_1_ = bf16[512,512]{1,0:T(8,128)(2,1)S(1)} collective-permute-done((bf16[512,512]{1,0:T(8,128)(2,1)S(1)}, bf16[512,512]{1,0:T(8,128)(2,1)S(1)}, u32[]{:S(2)}, u32[]{:S(2)}) %collective-permute-start.23) | collective-permute-done | bytes 524320 | tf_op jit(solution)/shard_map/ppermute | solution.py:384
  153.4 3.7 %collective-permute-done.25.refs_3_ = bf16[512,512]{1,0:T(8,128)(2,1)S(1)} collective-permute-done((bf16[512,512]{1,0:T(8,128)(2,1)S(1)}, bf16[512,512]{1,0:T(8,128)(2,1)S(1)}, u32[]{:S(2)}, u32[]{:S(2)}) %collective-permute-start.25) | collective-permute-done | bytes 524320 | tf_op jit(solution)/shard_map/ppermute | solution.py:384
  157.1 6.7 %collective-permute-done.28.refs_7_ = bf16[512,512]{1,0:T(8,128)(2,1)S(1)} collective-permute-done((bf16[512,512]{1,0:T(8,128)(2,1)S(1)}, bf16[512,512]{1,0:T(8,128)(2,1)S(1)}, u32[]{:S(2)}, u32[]{:S(2)}) %collective-permute-start.28) | collective-permute-done | bytes 524320 | tf_op jit(solution)/shard_map/ppermute | solution.py:384
  163.8 3.4 %relay.1 = (bf16[512,512]{1,0:T(8,128)(2,1)S(1)}, bf16[512,512]{1,0:T(8,128)(2,1)S(1)}, bf16[512,512]{1,0:T(8,128)(2,1)S(1)}, bf16[512,512]{1,0:T(8,128)(2,1)S(1...) custom-call(s32[2]{0:T(128)S(1)} %pad_add_fusion.place_ref, ...), custom_call_target="tpu_custom_call" | custom-call | flops 2147483648 | bytes 8388608 | tf_op jit(solution)/shard_map/relay/pallas_call | solution.py:345
  169.4 4.9 %collective-permute-start.32 = (bf16[512,512]{1,0:T(8,128)(2,1)S(1)}, bf16[512,512]{1,0:T(8,128)(2,1)S(1)}, u32[]{:S(2)}, u32[]{:S(2)}) collective-permute-start(bf16[512,512]{1,0:T(8,128)(2,1)S(1)} %get-tuple-element.72), channel_id=1, source_target_pairs={{0,192},{16,208},{32,224},{48,240},{64,0},{80,16},{96,32},{112,48}... | collective-permute-start | bytes 1572872 | tf_op jit(solution)/shard_map/ppermute | solution.py:384
  174.3 5.7 %collective-permute-done.29.refs_1_ = bf16[512,512]{1,0:T(8,128)(2,1)S(1)} collective-permute-done((bf16[512,512]{1,0:T(8,128)(2,1)S(1)}, bf16[512,512]{1,0:T(8,128)(2,1)S(1)}, u32[]{:S(2)}, u32[]{:S(2)}) %collective-permute-start.29) | collective-permute-done | bytes 524320 | tf_op jit(solution)/shard_map/ppermute | solution.py:384
  181.6 6.3 %collective-permute-done.30.refs_2_ = bf16[512,512]{1,0:T(8,128)(2,1)S(1)} collective-permute-done((bf16[512,512]{1,0:T(8,128)(2,1)S(1)}, bf16[512,512]{1,0:T(8,128)(2,1)S(1)}, u32[]{:S(2)}, u32[]{:S(2)}) %collective-permute-start.30) | collective-permute-done | bytes 524320 | tf_op jit(solution)/shard_map/ppermute | solution.py:384
  187.9 3.6 %collective-permute-done.32.refs_5_ = bf16[512,512]{1,0:T(8,128)(2,1)S(1)} collective-permute-done((bf16[512,512]{1,0:T(8,128)(2,1)S(1)}, bf16[512,512]{1,0:T(8,128)(2,1)S(1)}, u32[]{:S(2)}, u32[]{:S(2)}) %collective-permute-start.32) | collective-permute-done | bytes 524320 | tf_op jit(solution)/shard_map/ppermute | solution.py:384
  191.5 3.6 %collective-permute-done.33.refs_6_ = bf16[512,512]{1,0:T(8,128)(2,1)S(1)} collective-permute-done((bf16[512,512]{1,0:T(8,128)(2,1)S(1)}, bf16[512,512]{1,0:T(8,128)(2,1)S(1)}, u32[]{:S(2)}, u32[]{:S(2)}) %collective-permute-start.33) | collective-permute-done | bytes 524320 | tf_op jit(solution)/shard_map/ppermute | solution.py:384
  (82 shorter events, 53.7 us)
Async XLA Ops:
  21.1 16.1 %collective-permute-start.11 = (bf16[512,512]{1,0:T(8,128)(2,1)}, bf16[512,512]{1,0:T(8,128)(2,1)S(1)}, u32[]{:S(2)}, u32[]{:S(2)}) collective-permute-start(bf16[512,512]{1,0:T(8,128)(2,1)} %get-tuple-element.46.own_ref), channel_id=1, source_target_pairs={{0,48},{16,0},{32,16},{48,32},{64,112},{80,64},{96,80},{112,96},{1... | collective-permute-start | bytes 1572872 | tf_op jit(solution)/shard_map/ppermute | solution.py:384
  22.9 18.9 %collective-permute-start.15 = (bf16[512,512]{1,0:T(8,128)(2,1)}, bf16[512,512]{1,0:T(8,128)(2,1)}, u32[]{:S(2)}, u32[]{:S(2)}) collective-permute-start(bf16[512,512]{1,0:T(8,128)(2,1)} %get-tuple-element.50.own_ref), channel_id=1, source_target_pairs={{0,64},{16,80},{32,96},{48,112},{64,128},{80,144},{96,160},{112,17... | collective-permute-start | bytes 1572872 | tf_op jit(solution)/shard_map/ppermute | solution.py:384
  24.5 20.5 %collective-permute-start.17 = (bf16[512,512]{1,0:T(8,128)(2,1)}, bf16[512,512]{1,0:T(8,128)(2,1)}, u32[]{:S(2)}, u32[]{:S(2)}) collective-permute-start(bf16[512,512]{1,0:T(8,128)(2,1)} %get-tuple-element.50.own_ref), channel_id=1, source_target_pairs={{0,192},{16,208},{32,224},{48,240},{64,0},{80,16},{96,32},{112,48}... | collective-permute-start | bytes 1572872 | tf_op jit(solution)/shard_map/ppermute | solution.py:384
  31.6 42.4 %collective-permute-start.3 = (bf16[3,128,1024]{2,1,0:T(8,128)(2,1)S(1)}, bf16[3,128,1024]{2,1,0:T(8,128)(2,1)S(1)}, u32[]{:S(2)}, u32[]{:S(2)}) collective-permute-start(bf16[3,128,1024]{2,1,0:T(8,128)(2,1)S(1)} %collective-permute-done.2.refs_2_), channel_id=1, source_target_pairs={{0,2},{1,15},{2,4},{3,1},{4,6},{5,3},{6,8},{7,5},{8,10},{9,7},{10,... | collective-permute-start | bytes 2359304 | tf_op jit(solution)/shard_map/ppermute | solution.py:392
  38.8 23.8 %collective-permute-start.12 = (bf16[256,512]{1,0:T(8,128)(2,1)}, bf16[256,512]{1,0:T(8,128)(2,1)}, u32[]{:S(2)}, u32[]{:S(2)}) collective-permute-start(bf16[256,512]{1,0:T(8,128)(2,1)} %slice.22), channel_id=1, source_target_pairs={{0,48},{16,0},{32,16},{48,32},{64,112},{80,64},{96,80},{112,96},{1... | collective-permute-start | bytes 786440 | tf_op jit(solution)/shard_map/ppermute | solution.py:384
  43.4 26.2 %collective-permute-start.16 = (bf16[256,512]{1,0:T(8,128)(2,1)}, bf16[256,512]{1,0:T(8,128)(2,1)S(1)}, u32[]{:S(2)}, u32[]{:S(2)}) collective-permute-start(bf16[256,512]{1,0:T(8,128)(2,1)} %slice.23), channel_id=1, source_target_pairs={{0,64},{16,80},{32,96},{48,112},{64,128},{80,144},{96,160},{112,17... | collective-permute-start | bytes 786440 | tf_op jit(solution)/shard_map/ppermute | solution.py:384
  46.7 23.1 %collective-permute-start.18 = (bf16[256,512]{1,0:T(8,128)(2,1)}, bf16[256,512]{1,0:T(8,128)(2,1)}, u32[]{:S(2)}, u32[]{:S(2)}) collective-permute-start(bf16[256,512]{1,0:T(8,128)(2,1)} %slice.24), channel_id=1, source_target_pairs={{0,192},{16,208},{32,224},{48,240},{64,0},{80,16},{96,32},{112,48}... | collective-permute-start | bytes 786440 | tf_op jit(solution)/shard_map/ppermute | solution.py:384
  48.3 38.3 %collective-permute-start.5 = (bf16[3,128,1024]{2,1,0:T(8,128)(2,1)S(1)}, bf16[3,128,1024]{2,1,0:T(8,128)(2,1)}, u32[]{:S(2)}, u32[]{:S(2)}) collective-permute-start(bf16[3,128,1024]{2,1,0:T(8,128)(2,1)S(1)} %collective-permute-done.1.refs_1_), channel_id=1, source_target_pairs={{0,1},{1,0},{2,3},{3,2},{4,5},{5,4},{6,7},{7,6},{8,9},{9,8},{10,11... | collective-permute-start | bytes 2359304 | tf_op jit(solution)/shard_map/ppermute | solution.py:396
  69.6 20.3 %collective-permute-start.6 = (bf16[3,128,1024]{2,1,0:T(8,128)(2,1)S(1)}, bf16[3,128,1024]{2,1,0:T(8,128)(2,1)S(1)}, u32[]{:S(2)}, u32[]{:S(2)}) collective-permute-start(bf16[3,128,1024]{2,1,0:T(8,128)(2,1)S(1)} %collective-permute-done.2.refs_2_), channel_id=1, source_target_pairs={{0,1},{1,0},{2,3},{3,2},{4,5},{5,4},{6,7},{7,6},{8,9},{9,8},{10,11... | collective-permute-start | bytes 2359304 | tf_op jit(solution)/shard_map/ppermute | solution.py:396
  74.1 19.2 %collective-permute-start.7 = (bf16[3,128,1024]{2,1,0:T(8,128)(2,1)S(1)}, bf16[3,128,1024]{2,1,0:T(8,128)(2,1)S(1)}, u32[]{:S(2)}, u32[]{:S(2)}) collective-permute-start(bf16[3,128,1024]{2,1,0:T(8,128)(2,1)S(1)} %collective-permute-done.3.refs_3_), channel_id=1, source_target_pairs={{0,1},{1,0},{2,3},{3,2},{4,5},{5,4},{6,7},{7,6},{8,9},{9,8},{10,11... | collective-permute-start | bytes 2359304 | tf_op jit(solution)/shard_map/ppermute | solution.py:396
  83.9 25.8 %collective-permute-start.14 = (bf16[512,512]{1,0:T(8,128)(2,1)S(1)}, bf16[512,512]{1,0:T(8,128)(2,1)S(1)}, u32[]{:S(2)}, u32[]{:S(2)}) collective-permute-start(bf16[512,512]{1,0:T(8,128)(2,1)S(1)} %get-tuple-element.49), channel_id=1, source_target_pairs={{0,192},{16,208},{32,224},{48,240},{64,0},{80,16},{96,32},{112,48}... | collective-permute-start | bytes 1572872 | tf_op jit(solution)/shard_map/ppermute | solution.py:384
  86.6 23.1 %collective-permute-start.21 = (bf16[512,512]{1,0:T(8,128)(2,1)S(1)}, bf16[512,512]{1,0:T(8,128)(2,1)S(1)}, u32[]{:S(2)}, u32[]{:S(2)}) collective-permute-start(bf16[512,512]{1,0:T(8,128)(2,1)S(1)} %get-tuple-element.53), channel_id=1, source_target_pairs={{0,128},{16,144},{32,160},{48,176},{64,192},{80,208},{96,224},{112... | collective-permute-start | bytes 1572872 | tf_op jit(solution)/shard_map/ppermute | solution.py:384
  89.9 26.6 %collective-permute-start.19 = (bf16[512,512]{1,0:T(8,128)(2,1)S(1)}, bf16[512,512]{1,0:T(8,128)(2,1)S(1)}, u32[]{:S(2)}, u32[]{:S(2)}) collective-permute-start(bf16[512,512]{1,0:T(8,128)(2,1)S(1)} %get-tuple-element.51), channel_id=1, source_target_pairs={{0,16},{16,32},{32,48},{48,0},{64,80},{80,96},{96,112},{112,64},{1... | collective-permute-start | bytes 1572872 | tf_op jit(solution)/shard_map/ppermute | solution.py:384
  90.6 25.9 %collective-permute-start.20 = (bf16[512,512]{1,0:T(8,128)(2,1)S(1)}, bf16[512,512]{1,0:T(8,128)(2,1)S(1)}, u32[]{:S(2)}, u32[]{:S(2)}) collective-permute-start(bf16[512,512]{1,0:T(8,128)(2,1)S(1)} %get-tuple-element.52), channel_id=1, source_target_pairs={{0,48},{16,0},{32,16},{48,32},{64,112},{80,64},{96,80},{112,96},{1... | collective-permute-start | bytes 1572872 | tf_op jit(solution)/shard_map/ppermute | solution.py:384
  93.3 23.3 %collective-permute-start.22 = (bf16[512,512]{1,0:T(8,128)(2,1)S(1)}, bf16[512,512]{1,0:T(8,128)(2,1)S(1)}, u32[]{:S(2)}, u32[]{:S(2)}) collective-permute-start(bf16[512,512]{1,0:T(8,128)(2,1)S(1)} %get-tuple-element.56), channel_id=1, source_target_pairs={{0,32},{16,48},{32,0},{48,16},{64,96},{80,112},{96,64},{112,80},{1... | collective-permute-start | bytes 1572872 | tf_op jit(solution)/shard_map/ppermute | solution.py:384
  129.6 23.8 %collective-permute-start.23 = (bf16[512,512]{1,0:T(8,128)(2,1)S(1)}, bf16[512,512]{1,0:T(8,128)(2,1)S(1)}, u32[]{:S(2)}, u32[]{:S(2)}) collective-permute-start(bf16[512,512]{1,0:T(8,128)(2,1)S(1)} %get-tuple-element.60), channel_id=1, source_target_pairs={{0,192},{16,208},{32,224},{48,240},{64,0},{80,16},{96,32},{112,48}... | collective-permute-start | bytes 1572872 | tf_op jit(solution)/shard_map/ppermute | solution.py:384
  131.4 22.0 %collective-permute-start.24 = (bf16[512,512]{1,0:T(8,128)(2,1)S(1)}, bf16[512,512]{1,0:T(8,128)(2,1)S(1)}, u32[]{:S(2)}, u32[]{:S(2)}) collective-permute-start(bf16[512,512]{1,0:T(8,128)(2,1)S(1)} %get-tuple-element.61), channel_id=1, source_target_pairs={{0,128},{16,144},{32,160},{48,176},{64,192},{80,208},{96,224},{112... | collective-permute-start | bytes 1572872 | tf_op jit(solution)/shard_map/ppermute | solution.py:384
  133.0 24.0 %collective-permute-start.25 = (bf16[512,512]{1,0:T(8,128)(2,1)S(1)}, bf16[512,512]{1,0:T(8,128)(2,1)S(1)}, u32[]{:S(2)}, u32[]{:S(2)}) collective-permute-start(bf16[512,512]{1,0:T(8,128)(2,1)S(1)} %get-tuple-element.62), channel_id=1, source_target_pairs={{0,64},{16,80},{32,96},{48,112},{64,128},{80,144},{96,160},{112,17... | collective-permute-start | bytes 1572872 | tf_op jit(solution)/shard_map/ppermute | solution.py:384
  134.3 22.7 %collective-permute-start.26 = (bf16[512,512]{1,0:T(8,128)(2,1)S(1)}, bf16[512,512]{1,0:T(8,128)(2,1)S(1)}, u32[]{:S(2)}, u32[]{:S(2)}) collective-permute-start(bf16[512,512]{1,0:T(8,128)(2,1)S(1)} %get-tuple-element.64), channel_id=1, source_target_pairs={{0,48},{16,0},{32,16},{48,32},{64,112},{80,64},{96,80},{112,96},{1... | collective-permute-start | bytes 1572872 | tf_op jit(solution)/shard_map/ppermute | solution.py:384
  137.3 19.8 %collective-permute-start.27 = (bf16[512,512]{1,0:T(8,128)(2,1)S(1)}, bf16[512,512]{1,0:T(8,128)(2,1)S(1)}, u32[]{:S(2)}, u32[]{:S(2)}) collective-permute-start(bf16[512,512]{1,0:T(8,128)(2,1)S(1)} %get-tuple-element.65), channel_id=1, source_target_pairs={{0,32},{16,48},{32,0},{48,16},{64,96},{80,112},{96,64},{112,80},{1... | collective-permute-start | bytes 1572872 | tf_op jit(solution)/shard_map/ppermute | solution.py:384
  167.3 20.6 %collective-permute-start.30 = (bf16[512,512]{1,0:T(8,128)(2,1)S(1)}, bf16[512,512]{1,0:T(8,128)(2,1)S(1)}, u32[]{:S(2)}, u32[]{:S(2)}) collective-permute-start(bf16[512,512]{1,0:T(8,128)(2,1)S(1)} %get-tuple-element.69), channel_id=1, source_target_pairs={{0,16},{16,32},{32,48},{48,0},{64,80},{80,96},{96,112},{112,64},{1... | collective-permute-start | bytes 1572872 | tf_op jit(solution)/shard_map/ppermute | solution.py:384
  169.3 18.6 %collective-permute-start.31 = (bf16[512,512]{1,0:T(8,128)(2,1)S(1)}, bf16[512,512]{1,0:T(8,128)(2,1)S(1)}, u32[]{:S(2)}, u32[]{:S(2)}) collective-permute-start(bf16[512,512]{1,0:T(8,128)(2,1)S(1)} %get-tuple-element.70), channel_id=1, source_target_pairs={{0,32},{16,48},{32,0},{48,16},{64,96},{80,112},{96,64},{112,80},{1... | collective-permute-start | bytes 1572872 | tf_op jit(solution)/shard_map/ppermute | solution.py:384
  169.4 22.1 %collective-permute-start.32 = (bf16[512,512]{1,0:T(8,128)(2,1)S(1)}, bf16[512,512]{1,0:T(8,128)(2,1)S(1)}, u32[]{:S(2)}, u32[]{:S(2)}) collective-permute-start(bf16[512,512]{1,0:T(8,128)(2,1)S(1)} %get-tuple-element.72), channel_id=1, source_target_pairs={{0,192},{16,208},{32,224},{48,240},{64,0},{80,16},{96,32},{112,48}... | collective-permute-start | bytes 1572872 | tf_op jit(solution)/shard_map/ppermute | solution.py:384
  174.3 20.8 %collective-permute-start.33 = (bf16[512,512]{1,0:T(8,128)(2,1)S(1)}, bf16[512,512]{1,0:T(8,128)(2,1)S(1)}, u32[]{:S(2)}, u32[]{:S(2)}) collective-permute-start(bf16[512,512]{1,0:T(8,128)(2,1)S(1)} %get-tuple-element.73), channel_id=1, source_target_pairs={{0,64},{16,80},{32,96},{48,112},{64,128},{80,144},{96,160},{112,17... | collective-permute-start | bytes 1572872 | tf_op jit(solution)/shard_map/ppermute | solution.py:384
  (20 other events, 183.7 us)

commit v3 on v2

--- a/solution.py
+++ b/solution.py
@@ -61,13 +61,18 @@
     )(bounds, listed.reshape(-1, slots), affinity.reshape(-1, slots))
 
 
-def prepare_kernel(stream_ref, gain_ref, gate_ref, up_ref, down_ref, low_ref, high_ref, piece_ref):
+def prepare_kernel(stream_ref, gain_ref, gate_ref, up_ref, down_ref, *refs):
     values = stream_ref[...].astype(jnp.float32)
     inverse = lax.rsqrt(jnp.mean(values * values, axis=-1, keepdims=True) + epsilon)
     normed = (values * inverse * gain_ref[...]).astype(jnp.bfloat16)
-    half = low_ref.shape[1]
-    low_ref[...] = normed[:, :half]
+    high_ref, piece_ref = refs[2:]
+    half = high_ref.shape[1]
     high_ref[...] = normed[:, half:]
+    for part in range(2):
+
+        @pl.when(pl.program_id(0) == part)
+        def _():
+            refs[part][...] = normed[:, :half]
 
     @pl.when(pl.program_id(0) == 0)
     def _():
@@ -92,12 +97,12 @@
             part,
         ],
         out_specs=(
-            pl.BlockSpec((step, half), lambda i: (i, 0)),
+            *[pl.BlockSpec((step, half), lambda i: (0, 0))] * 2,
             pl.BlockSpec((step, half), lambda i: (i, 0)),
             pl.BlockSpec(piece, lambda i: (0, 0, 0)),
         ),
         out_shape=(
-            jax.ShapeDtypeStruct((rows, half), jnp.bfloat16),
+            *[jax.ShapeDtypeStruct((step, half), jnp.bfloat16)] * 2,
             jax.ShapeDtypeStruct((rows, half), jnp.bfloat16),
             jax.ShapeDtypeStruct(piece, jnp.bfloat16),
         ),
@@ -106,14 +111,16 @@
     )(stream, norm_gain.reshape(1, features), *parts)
 
 
-def pick_kernel(along_y, place_ref, rows_ref, own_ref, after_ref, top_ref, bottom_ref, before_ref, *refs):
-    outs = refs[:SIDE]
-    across_ref, chosen_ref = refs[SIDE:]
+def pick_kernel(along_y, place_ref, rows_ref, *refs):
+    sources, outs = refs[: -SIDE - 2], refs[-SIDE - 2 : -2]
+    sources_ref, chosen_ref = refs[-2:]
     y, x = place_ref[0], place_ref[1]
-    tokens, half = own_ref.shape
+    _, tokens, half = sources_ref.shape
     slots = rows_ref.shape[2]
-    across_ref[: tokens // 2, :] = top_ref[...]
-    across_ref[tokens // 2 :, :] = bottom_ref[...]
+    at = 0
+    for source in sources:
+        sources_ref[at // tokens, at % tokens : at % tokens + source.shape[0], :] = source[...]
+        at += source.shape[0]
     token = lax.broadcasted_iota(jnp.int32, (slots, tokens), 1).astype(jnp.float32)
     for d in range(SIDE):
         e = wrap(y + d) * SIDE + x if along_y else y * SIDE + wrap(x + d)
@@ -127,8 +134,8 @@
 
     def work(i, carry):
         at = pl.ds(pl.multiple_of(i * step, step), step)
-        for t, source in enumerate((own_ref, after_ref, across_ref, before_ref)):
-            rows = jnp.dot(chosen_ref[t], source[:, at], preferred_element_type=jnp.float32).astype(jnp.bfloat16)
+        for t in range(SIDE):
+            rows = jnp.dot(chosen_ref[t], sources_ref[t, :, at], preferred_element_type=jnp.float32).astype(jnp.bfloat16)
             for d in range(SIDE):
                 outs[d][t * slots : (t + 1) * slots, at] = rows[d * slots : (d + 1) * slots, :]
         return carry
@@ -137,14 +144,14 @@
 
 
 def pick(along_y, place, rows, sources):
-    tokens, half = sources[0].shape
+    tokens, half = sum(source.shape[0] for source in sources) // SIDE, sources[0].shape[1]
     slots = rows.shape[2]
     return pl.pallas_call(
         functools.partial(pick_kernel, along_y),
-        in_specs=[SMEM] + [VMEM] * 6,
+        in_specs=[SMEM] + [VMEM] * (1 + len(sources)),
         out_shape=[jax.ShapeDtypeStruct((SIDE * slots, half), jnp.bfloat16)] * SIDE,
         scratch_shapes=[
-            pltpu.VMEM((tokens, half), jnp.bfloat16),
+            pltpu.VMEM((SIDE, tokens, half), jnp.bfloat16),
             pltpu.VMEM((SIDE, SIDE * slots, tokens), jnp.bfloat16),
         ],
         cost_estimate=pl.CostEstimate(
@@ -404,15 +411,15 @@
     ep_index = lax.axis_index("ep").astype(jnp.int32)
     place = jnp.stack([ep_index // SIDE, ep_index % SIDE])
     bounds = (jnp.arange(ep_count, dtype=jnp.int32) * tp_count + lax.axis_index("tp")) * block
-    low, high, own = prepare(stream, norm_gain, (gate_rows, up_rows, down_rows))
-    left, right = over_plane(low, 0, 1), over_plane(low, 0, -1)
+    *low, high, own = prepare(stream, norm_gain, (gate_rows, up_rows, down_rows))
+    left, right = [over_plane(part, 0, 1) for part in low], [over_plane(part, 0, -1) for part in low]
     down, up = over_plane(high, 1, 0), over_plane(high, -1, 0)
     both = stack([own, other_core(own, tp_count)])
     next1 = along_z(both, 1, tp_count)
     rows_there, weights = windows(bounds, chosen, affinity, block, slots)
     rows_here = lax.all_to_all(rows_there, "ep", split_axis=0, concat_axis=0, tiled=True)
+    lows = [*low, *left, over_plane(left[0], 0, 1), over_plane(right[1], 0, -1), *right]
     mid = block // 2
-    lows = [low, left, over_plane(left[:mid], 0, 1), over_plane(right[mid:], 0, -1), right]
     highs = [high, down, over_plane(down[:mid], 1, 0), over_plane(up[mid:], -1, 0), up]
     next2 = along_z(next1, 1, tp_count)
     picked_low = pick(True, place, rows_here, lows)

time: 197 us -> 199 us (1.010)
  the two profiles are of different devices: /device:TPU:32 before, /device:TPU:6 now
where the time goes in v3:
time: 199 us; the launch traced here: 198 us
  waiting for transfers between devices  98.8 us (50%)
  starting transfers between devices  56.8 us (29%)
  Pallas kernels  36.7 us (18%)
  local copies, waits for them, and re-layouts  5.36 us (3%)
    ppermute x28, waiting for transfers between devices, over_plane(): lax.ppermute(array, 'ep', [(y * SIDE + x, (y + by_y) % SIDE * SIDE + (x +...  56.2 us
    ppermute x28, starting transfers between devices, over_plane(): lax.ppermute(array, 'ep', [(y * SIDE + x, (y + by_y) % SIDE * SIDE + (x +...  46.5 us
    ppermute x4, waiting for transfers between devices, along_z(): lax.ppermute(array, 'tp', [(z * 2 + c, to * 2 + c) for z, c, to in pairs])  35 us
    pallas_call x3, Pallas kernels, expert(): pl.pallas_call(functools.partial(expert_kernel, number, [*inputs, *outs])...  17.6 us
    all_to_all x1, starting transfers between devices, layer(): lax.all_to_all(rows_there, 'ep', split_axis=0, concat_axis=0, tiled=True)  7.24 us
    pallas_call x2, Pallas kernels, pick(): pl.pallas_call(functools.partial(pick_kernel, along_y), in_specs=[SMEM] +...  6.88 us
    all_to_all x1, waiting for transfers between devices, layer(): lax.all_to_all(rows_there, 'ep', split_axis=0, concat_axis=0, tiled=True)  5.62 us
  transfers between devices with their start and end apart: 38, of which 22 were waited for; matrix products, arithmetic and copies ran while one was open for 2% of the time, Pallas kernels for 8%

profile of v3, /device:TPU:6, one launch (start us, length us, event | category | flops | bytes accessed | tf_op | source)
XLA Modules:
  0.0 198.3 jit_solution(8245161988636806620)
XLA Ops:
  0.0 2.7 %prepare.1 = (bf16[256,512]{1,0:T(8,128)(2,1)}, bf16[256,512]{1,0:T(8,128)(2,1)}, bf16[512,512]{1,0:T(8,128)(2,1)}, bf16[3,64,1024]{2,1,0:T(8,128)(2,1)}) custom-call(bf16[512,1024]{1,0:T(8,128)(2,1)} %stream_ref.1, f32[1,1024]{1,0:T(1,128)} %bitcast.7, bf16[1,64,1024]{2,1,0:T(8,128)(2,1)} %gate_ref.1, bf16[1,64,1024]{2,1,0:T(8,128)(2,1)} %up_ref.1, ...), custom_call_target="tpu_custom_call" | custom-call | flops 3000000 | bytes 3145728 | tf_op jit(solution)/shard_map/prepare/pallas_call | solution.py:89
  7.7 13.9 %collective-permute-done.1.refs_1_ = bf16[3,128,1024]{2,1,0:T(8,128)(2,1)S(1)} collective-permute-done((bf16[3,128,1024]{2,1,0:T(8,128)(2,1)S(1)}, bf16[3,128,1024]{2,1,0:T(8,128)(2,1)S(1)}, u32[]{:S(2)}, u32[]{:S(2)}) %collective-permute-start.1) | collective-permute-done | bytes 786464 | tf_op jit(solution)/shard_map/ppermute | solution.py:399
  26.9 7.9 %collective-permute-done.2.refs_2_ = bf16[3,128,1024]{2,1,0:T(8,128)(2,1)S(1)} collective-permute-done((bf16[3,128,1024]{2,1,0:T(8,128)(2,1)S(1)}, bf16[3,128,1024]{2,1,0:T(8,128)(2,1)S(1)}, u32[]{:S(2)}, u32[]{:S(2)}) %collective-permute-start.2) | collective-permute-done | bytes 786464 | tf_op jit(solution)/shard_map/ppermute | solution.py:399
  53.1 7.2 %all-to-all-start = ((s32[16,8,128]{2,1,0:T(8,128)}), s32[16,8,128]{2,1,0:T(8,128)S(1)}, u32[]{:S(2)}, u32[]{:S(2)}) async-start(s32[16,8,128]{2,1,0:T(8,128)} %get-tuple-element.41), calls=%async_computation | async-start | bytes 131072 | tf_op jit(solution)/shard_map/all_to_all | solution.py:420
  60.5 5.6 %all-to-all-done.rows_ref = s32[16,8,128]{2,1,0:T(8,128)S(1)} async-done(((s32[16,8,128]{2,1,0:T(8,128)}), s32[16,8,128]{2,1,0:T(8,128)S(1)}, u32[]{:S(2)}, u32[]{:S(2)}) %all-to-all-start) | async-done | bytes 65568 | tf_op jit(solution)/shard_map/all_to_all | solution.py:420
  67.1 3.4 %pick_y.1 = (bf16[512,512]{1,0:T(8,128)(2,1)S(1)}, bf16[512,512]{1,0:T(8,128)(2,1)S(1)}, bf16[512,512]{1,0:T(8,128)(2,1)S(1)}, bf16[512,512]{1,0:T(8,128)(2,1)S(1)}) custom-call(s32[2]{0:T(128)S(1)} %pad_add_fusion.place_ref, s32[16,8,128]{2,1,0:T(8,128)S(1)} %all-to-all-done.rows_ref, bf16[256,512]{1,0:T(8,128)(2,1)S(1)} %copy-done.2, ...), custom_call_target="tpu_custom_call" | custom-call | flops 1073741824 | bytes 4194304 | tf_op jit(solution)/shard_map/pick_y/pallas_call | solution.py:149
  71.9 13.2 %collective-permute-done.4.refs_4_ = bf16[3,64,1024]{2,1,0:T(8,128)(2,1)S(1)} collective-permute-done((bf16[3,64,1024]{2,1,0:T(8,128)(2,1)S(1)}, bf16[3,64,1024]{2,1,0:T(8,128)(2,1)S(1)}, u32[]{:S(2)}, u32[]{:S(2)}) %collective-permute-start.4) | collective-permute-done | bytes 393248 | tf_op jit(solution)/shard_map/ppermute | solution.py:399
  85.1 2.7 %collective-permute-start.16 = (bf16[512,512]{1,0:T(8,128)(2,1)S(1)}, bf16[512,512]{1,0:T(8,128)(2,1)S(1)}, u32[]{:S(2)}, u32[]{:S(2)}) collective-permute-start(bf16[512,512]{1,0:T(8,128)(2,1)S(1)} %get-tuple-element.51), channel_id=1, source_target_pairs={{0,192},{16,208},{32,224},{48,240},{64,0},{80,16},{96,32},{112,48}... | collective-permute-start | bytes 1572872 | tf_op jit(solution)/shard_map/ppermute | solution.py:391
  87.8 3.4 %pick_x.1 = (bf16[512,512]{1,0:T(8,128)(2,1)S(1)}, bf16[512,512]{1,0:T(8,128)(2,1)S(1)}, bf16[512,512]{1,0:T(8,128)(2,1)S(1)}, bf16[512,512]{1,0:T(8,128)(2,1)S(1)}) custom-call(s32[2]{0:T(128)S(1)} %pad_add_fusion.place_ref, s32[16,8,128]{2,1,0:T(8,128)S(1)} %all-to-all-done.rows_ref, bf16[512,512]{1,0:T(8,128)(2,1)S(1)} %copy-done.1, ...), custom_call_target="tpu_custom_call" | custom-call | flops 1073741824 | bytes 4194304 | tf_op jit(solution)/shard_map/pick_x/pallas_call | solution.py:149
  97.1 13.8 %collective-permute-done.16.refs_3_.refs_2_ = bf16[512,512]{1,0:T(8,128)(2,1)S(1)} collective-permute-done((bf16[512,512]{1,0:T(8,128)(2,1)S(1)}, bf16[512,512]{1,0:T(8,128)(2,1)S(1)}, u32[]{:S(2)}, u32[]{:S(2)}) %collective-permute-start.16) | collective-permute-done | bytes 524320 | tf_op jit(solution)/shard_map/ppermute | solution.py:391
  110.9 4.5 %shard_map.74 = (bf16[512,512]{1,0:T(8,128)(2,1)S(1)}, bf16[512,512]{1,0:T(8,128)(2,1)S(1)}) custom-call(s32[2]{0:T(128)S(1)} %pad_add_fusion.place_ref, f32[16,128]{1,0:T(8,128)S(1)} %copy-done.4, bf16[1024,1024]{1,0:T(8,128)(2,1)S(1)} %get-tuple-element.44.gate_ref, bf16[1024,1024]{1,0:T(8,128)(2,1)S(1)} %get-tuple-element.45.up_ref, ...), custom_call_target="tpu_custom_call" | custom-call | flops 3221225472 | bytes 2097152 | tf_op jit(solution)/shard_map/pallas_call | solution.py:303
  116.3 3.4 %collective-permute-done.22.refs_6_.refs_4_ = bf16[512,512]{1,0:T(8,128)(2,1)S(1)} collective-permute-done((bf16[512,512]{1,0:T(8,128)(2,1)S(1)}, bf16[512,512]{1,0:T(8,128)(2,1)S(1)}, u32[]{:S(2)}, u32[]{:S(2)}) %collective-permute-start.22) | collective-permute-done | bytes 524320 | tf_op jit(solution)/shard_map/ppermute | solution.py:391
  119.6 6.5 %shard_map.75 = (bf16[512,512]{1,0:T(8,128)(2,1)S(1)}, bf16[512,512]{1,0:T(8,128)(2,1)S(1)}, bf16[768,512]{1,0:T(8,128)(2,1)S(1)}, bf16[768,512]{1,0:T(8,128)(2,1)S(1)}) custom-call(s32[2]{0:T(128)S(1)} %pad_add_fusion.place_ref, f32[16,128]{1,0:T(8,128)S(1)} %copy-done.4, bf16[1024,1024]{1,0:T(8,128)(2,1)S(1)} %get-tuple-element.44.gate_ref, ...), custom_call_target="tpu_custom_call" | custom-call | flops 4831838208 | bytes 3145728 | tf_op jit(solution)/shard_map/pallas_call | solution.py:303
  126.2 6.5 %shard_map.76 = (bf16[512,512]{1,0:T(8,128)(2,1)S(1)}, bf16[512,512]{1,0:T(8,128)(2,1)S(1)}, bf16[512,512]{1,0:T(8,128)(2,1)S(1)}, bf16[512,512]{1,0:T(8,128)(2,1)S(1)}, bf16[512,512]{1,0:T(8,128)(2,1)S(1)}) custom-call(s32[2]{0:T(128)S(1)} %pad_add_fusion.place_ref, f32[16,128]{1,0:T(8,128)S(1)} %copy-done.4, ...), custom_call_target="tpu_custom_call" | custom-call | flops 4831838208 | bytes 3145728 | tf_op jit(solution)/shard_map/pallas_call | solution.py:303
  139.2 8.4 %collective-permute-done.25.refs_1_ = bf16[512,512]{1,0:T(8,128)(2,1)S(1)} collective-permute-done((bf16[512,512]{1,0:T(8,128)(2,1)S(1)}, bf16[512,512]{1,0:T(8,128)(2,1)S(1)}, u32[]{:S(2)}, u32[]{:S(2)}) %collective-permute-start.25) | collective-permute-done | bytes 524320 | tf_op jit(solution)/shard_map/ppermute | solution.py:391
  147.6 9.0 %collective-permute-start.30 = (bf16[512,512]{1,0:T(8,128)(2,1)S(1)}, bf16[512,512]{1,0:T(8,128)(2,1)S(1)}, u32[]{:S(2)}, u32[]{:S(2)}) collective-permute-start(bf16[512,512]{1,0:T(8,128)(2,1)S(1)} %get-tuple-element.68), channel_id=1, source_target_pairs={{0,16},{16,32},{32,48},{48,0},{64,80},{80,96},{96,112},{112,64},{1... | collective-permute-start | bytes 1572872 | tf_op jit(solution)/shard_map/ppermute | solution.py:391
  160.6 2.7 %collective-permute-done.30.refs_7_ = bf16[512,512]{1,0:T(8,128)(2,1)S(1)} collective-permute-done((bf16[512,512]{1,0:T(8,128)(2,1)S(1)}, bf16[512,512]{1,0:T(8,128)(2,1)S(1)}, u32[]{:S(2)}, u32[]{:S(2)}) %collective-permute-start.30) | collective-permute-done | bytes 524320 | tf_op jit(solution)/shard_map/ppermute | solution.py:391
  163.3 3.4 %relay.1 = (bf16[512,512]{1,0:T(8,128)(2,1)S(1)}, bf16[512,512]{1,0:T(8,128)(2,1)S(1)}, bf16[512,512]{1,0:T(8,128)(2,1)S(1)}, bf16[512,512]{1,0:T(8,128)(2,1)S(1...) custom-call(s32[2]{0:T(128)S(1)} %pad_add_fusion.place_ref, ...), custom_call_target="tpu_custom_call" | custom-call | flops 2147483648 | bytes 8388608 | tf_op jit(solution)/shard_map/relay/pallas_call | solution.py:352
  167.9 2.9 %collective-permute-start.32 = (bf16[512,512]{1,0:T(8,128)(2,1)S(1)}, bf16[512,512]{1,0:T(8,128)(2,1)S(1)}, u32[]{:S(2)}, u32[]{:S(2)}) collective-permute-start(bf16[512,512]{1,0:T(8,128)(2,1)S(1)} %get-tuple-element.71), channel_id=1, source_target_pairs={{0,16},{16,32},{32,48},{48,0},{64,80},{80,96},{96,112},{112,64},{1... | collective-permute-start | bytes 1572872 | tf_op jit(solution)/shard_map/ppermute | solution.py:391
  172.0 4.8 %collective-permute-start.34 = (bf16[512,512]{1,0:T(8,128)(2,1)S(1)}, bf16[512,512]{1,0:T(8,128)(2,1)S(1)}, u32[]{:S(2)}, u32[]{:S(2)}) collective-permute-start(bf16[512,512]{1,0:T(8,128)(2,1)S(1)} %get-tuple-element.74), channel_id=1, source_target_pairs={{0,192},{16,208},{32,224},{48,240},{64,0},{80,16},{96,32},{112,48}... | collective-permute-start | bytes 1572872 | tf_op jit(solution)/shard_map/ppermute | solution.py:391
  176.8 5.9 %collective-permute-done.31.refs_1_ = bf16[512,512]{1,0:T(8,128)(2,1)S(1)} collective-permute-done((bf16[512,512]{1,0:T(8,128)(2,1)S(1)}, bf16[512,512]{1,0:T(8,128)(2,1)S(1)}, u32[]{:S(2)}, u32[]{:S(2)}) %collective-permute-start.31) | collective-permute-done | bytes 524320 | tf_op jit(solution)/shard_map/ppermute | solution.py:391
  182.8 4.9 %collective-permute-done.32.refs_2_ = bf16[512,512]{1,0:T(8,128)(2,1)S(1)} collective-permute-done((bf16[512,512]{1,0:T(8,128)(2,1)S(1)}, bf16[512,512]{1,0:T(8,128)(2,1)S(1)}, u32[]{:S(2)}, u32[]{:S(2)}) %collective-permute-start.32) | collective-permute-done | bytes 524320 | tf_op jit(solution)/shard_map/ppermute | solution.py:391
  188.4 5.4 %collective-permute-done.34.refs_5_ = bf16[512,512]{1,0:T(8,128)(2,1)S(1)} collective-permute-done((bf16[512,512]{1,0:T(8,128)(2,1)S(1)}, bf16[512,512]{1,0:T(8,128)(2,1)S(1)}, u32[]{:S(2)}, u32[]{:S(2)}) %collective-permute-start.34) | collective-permute-done | bytes 524320 | tf_op jit(solution)/shard_map/ppermute | solution.py:391
  193.8 2.8 %collective-permute-done.35.refs_6_ = bf16[512,512]{1,0:T(8,128)(2,1)S(1)} collective-permute-done((bf16[512,512]{1,0:T(8,128)(2,1)S(1)}, bf16[512,512]{1,0:T(8,128)(2,1)S(1)}, u32[]{:S(2)}, u32[]{:S(2)}) %collective-permute-start.35) | collective-permute-done | bytes 524320 | tf_op jit(solution)/shard_map/ppermute | solution.py:391
  (78 shorter events, 52.9 us)
Async XLA Ops:
  5.7 15.9 %collective-permute-start.1 = (bf16[3,128,1024]{2,1,0:T(8,128)(2,1)S(1)}, bf16[3,128,1024]{2,1,0:T(8,128)(2,1)S(1)}, u32[]{:S(2)}, u32[]{:S(2)}) collective-permute-start(bf16[3,128,1024]{2,1,0:T(8,128)(2,1)S(1)} %shard_map.73.refs_0_), channel_id=1, source_target_pairs={{0,2},{1,15},{2,4},{3,1},{4,6},{5,3},{6,8},{7,5},{8,10},{9,7},{10,... | collective-permute-start | bytes 2359304 | tf_op jit(solution)/shard_map/ppermute | solution.py:399
  23.2 15.9 %collective-permute-start.19 = (bf16[512,512]{1,0:T(8,128)(2,1)}, bf16[512,512]{1,0:T(8,128)(2,1)}, u32[]{:S(2)}, u32[]{:S(2)}) collective-permute-start(bf16[512,512]{1,0:T(8,128)(2,1)} %get-tuple-element.52.refs_0_), channel_id=1, source_target_pairs={{0,192},{16,208},{32,224},{48,240},{64,0},{80,16},{96,32},{112,48}... | collective-permute-start | bytes 1572872 | tf_op jit(solution)/shard_map/ppermute | solution.py:391
  34.8 36.6 %collective-permute-start.3 = (bf16[3,128,1024]{2,1,0:T(8,128)(2,1)S(1)}, bf16[3,128,1024]{2,1,0:T(8,128)(2,1)S(1)}, u32[]{:S(2)}, u32[]{:S(2)}) collective-permute-start(bf16[3,128,1024]{2,1,0:T(8,128)(2,1)S(1)} %collective-permute-done.2.refs_2_), channel_id=1, source_target_pairs={{0,2},{1,15},{2,4},{3,1},{4,6},{5,3},{6,8},{7,5},{8,10},{9,7},{10,... | collective-permute-start | bytes 2359304 | tf_op jit(solution)/shard_map/ppermute | solution.py:399
  39.1 27.0 %collective-permute-start.13 = (bf16[256,512]{1,0:T(8,128)(2,1)}, bf16[256,512]{1,0:T(8,128)(2,1)}, u32[]{:S(2)}, u32[]{:S(2)}) collective-permute-start(bf16[256,512]{1,0:T(8,128)(2,1)} %collective-permute-done.12.refs_7_), channel_id=1, source_target_pairs={{0,48},{16,0},{32,16},{48,32},{64,112},{80,64},{96,80},{112,96},{1... | collective-permute-start | bytes 786440 | tf_op jit(solution)/shard_map/ppermute | solution.py:391
  44.1 27.1 %collective-permute-start.18 = (bf16[256,512]{1,0:T(8,128)(2,1)}, bf16[256,512]{1,0:T(8,128)(2,1)}, u32[]{:S(2)}, u32[]{:S(2)}) collective-permute-start(bf16[256,512]{1,0:T(8,128)(2,1)} %slice.13), channel_id=1, source_target_pairs={{0,64},{16,80},{32,96},{48,112},{64,128},{80,144},{96,160},{112,17... | collective-permute-start | bytes 786440 | tf_op jit(solution)/shard_map/ppermute | solution.py:391
  46.6 24.8 %collective-permute-start.20 = (bf16[256,512]{1,0:T(8,128)(2,1)}, bf16[256,512]{1,0:T(8,128)(2,1)}, u32[]{:S(2)}, u32[]{:S(2)}) collective-permute-start(bf16[256,512]{1,0:T(8,128)(2,1)} %slice.14), channel_id=1, source_target_pairs={{0,192},{16,208},{32,224},{48,240},{64,0},{80,16},{96,32},{112,48}... | collective-permute-start | bytes 786440 | tf_op jit(solution)/shard_map/ppermute | solution.py:391
  49.7 38.1 %collective-permute-start.5 = (bf16[3,128,1024]{2,1,0:T(8,128)(2,1)S(1)}, bf16[3,128,1024]{2,1,0:T(8,128)(2,1)}, u32[]{:S(2)}, u32[]{:S(2)}) collective-permute-start(bf16[3,128,1024]{2,1,0:T(8,128)(2,1)S(1)} %collective-permute-done.1.refs_1_), channel_id=1, source_target_pairs={{0,1},{1,0},{2,3},{3,2},{4,5},{5,4},{6,7},{7,6},{8,9},{9,8},{10,11... | collective-permute-start | bytes 2359304 | tf_op jit(solution)/shard_map/ppermute | solution.py:403
  71.2 20.0 %collective-permute-start.6 = (bf16[3,128,1024]{2,1,0:T(8,128)(2,1)S(1)}, bf16[3,128,1024]{2,1,0:T(8,128)(2,1)S(1)}, u32[]{:S(2)}, u32[]{:S(2)}) collective-permute-start(bf16[3,128,1024]{2,1,0:T(8,128)(2,1)S(1)} %collective-permute-done.2.refs_2_), channel_id=1, source_target_pairs={{0,1},{1,0},{2,3},{3,2},{4,5},{5,4},{6,7},{7,6},{8,9},{9,8},{10,11... | collective-permute-start | bytes 2359304 | tf_op jit(solution)/shard_map/ppermute | solution.py:403
  71.4 22.0 %collective-permute-start.7 = (bf16[3,128,1024]{2,1,0:T(8,128)(2,1)S(1)}, bf16[3,128,1024]{2,1,0:T(8,128)(2,1)S(1)}, u32[]{:S(2)}, u32[]{:S(2)}) collective-permute-start(bf16[3,128,1024]{2,1,0:T(8,128)(2,1)S(1)} %collective-permute-done.3.refs_3_), channel_id=1, source_target_pairs={{0,1},{1,0},{2,3},{3,2},{4,5},{5,4},{6,7},{7,6},{8,9},{9,8},{10,11... | collective-permute-start | bytes 2359304 | tf_op jit(solution)/shard_map/ppermute | solution.py:403
  85.1 25.8 %collective-permute-start.16 = (bf16[512,512]{1,0:T(8,128)(2,1)S(1)}, bf16[512,512]{1,0:T(8,128)(2,1)S(1)}, u32[]{:S(2)}, u32[]{:S(2)}) collective-permute-start(bf16[512,512]{1,0:T(8,128)(2,1)S(1)} %get-tuple-element.51), channel_id=1, source_target_pairs={{0,192},{16,208},{32,224},{48,240},{64,0},{80,16},{96,32},{112,48}... | collective-permute-start | bytes 1572872 | tf_op jit(solution)/shard_map/ppermute | solution.py:391
  87.8 23.1 %collective-permute-start.23 = (bf16[512,512]{1,0:T(8,128)(2,1)S(1)}, bf16[512,512]{1,0:T(8,128)(2,1)S(1)}, u32[]{:S(2)}, u32[]{:S(2)}) collective-permute-start(bf16[512,512]{1,0:T(8,128)(2,1)S(1)} %get-tuple-element.55), channel_id=1, source_target_pairs={{0,128},{16,144},{32,160},{48,176},{64,192},{80,208},{96,224},{112... | collective-permute-start | bytes 1572872 | tf_op jit(solution)/shard_map/ppermute | solution.py:391
  91.3 25.0 %collective-permute-start.21 = (bf16[512,512]{1,0:T(8,128)(2,1)S(1)}, bf16[512,512]{1,0:T(8,128)(2,1)S(1)}, u32[]{:S(2)}, u32[]{:S(2)}) collective-permute-start(bf16[512,512]{1,0:T(8,128)(2,1)S(1)} %get-tuple-element.53), channel_id=1, source_target_pairs={{0,16},{16,32},{32,48},{48,0},{64,80},{80,96},{96,112},{112,64},{1... | collective-permute-start | bytes 1572872 | tf_op jit(solution)/shard_map/ppermute | solution.py:391
  93.4 26.2 %collective-permute-start.22 = (bf16[512,512]{1,0:T(8,128)(2,1)S(1)}, bf16[512,512]{1,0:T(8,128)(2,1)S(1)}, u32[]{:S(2)}, u32[]{:S(2)}) collective-permute-start(bf16[512,512]{1,0:T(8,128)(2,1)S(1)} %get-tuple-element.54), channel_id=1, source_target_pairs={{0,48},{16,0},{32,16},{48,32},{64,112},{80,64},{96,80},{112,96},{1... | collective-permute-start | bytes 1572872 | tf_op jit(solution)/shard_map/ppermute | solution.py:391
  93.4 26.2 %collective-permute-start.24 = (bf16[512,512]{1,0:T(8,128)(2,1)S(1)}, bf16[512,512]{1,0:T(8,128)(2,1)S(1)}, u32[]{:S(2)}, u32[]{:S(2)}) collective-permute-start(bf16[512,512]{1,0:T(8,128)(2,1)S(1)} %get-tuple-element.58), channel_id=1, source_target_pairs={{0,32},{16,48},{32,0},{48,16},{64,96},{80,112},{96,64},{112,80},{1... | collective-permute-start | bytes 1572872 | tf_op jit(solution)/shard_map/ppermute | solution.py:391
  134.5 22.1 %collective-permute-start.26 = (bf16[512,512]{1,0:T(8,128)(2,1)S(1)}, bf16[512,512]{1,0:T(8,128)(2,1)S(1)}, u32[]{:S(2)}, u32[]{:S(2)}) collective-permute-start(bf16[512,512]{1,0:T(8,128)(2,1)S(1)} %get-tuple-element.63), channel_id=1, source_target_pairs={{0,128},{16,144},{32,160},{48,176},{64,192},{80,208},{96,224},{112... | collective-permute-start | bytes 1572872 | tf_op jit(solution)/shard_map/ppermute | solution.py:391
  136.1 22.4 %collective-permute-start.27 = (bf16[512,512]{1,0:T(8,128)(2,1)S(1)}, bf16[512,512]{1,0:T(8,128)(2,1)S(1)}, u32[]{:S(2)}, u32[]{:S(2)}) collective-permute-start(bf16[512,512]{1,0:T(8,128)(2,1)S(1)} %get-tuple-element.64), channel_id=1, source_target_pairs={{0,64},{16,80},{32,96},{48,112},{64,128},{80,144},{96,160},{112,17... | collective-permute-start | bytes 1572872 | tf_op jit(solution)/shard_map/ppermute | solution.py:391
  137.5 23.1 %collective-permute-start.28 = (bf16[512,512]{1,0:T(8,128)(2,1)S(1)}, bf16[512,512]{1,0:T(8,128)(2,1)S(1)}, u32[]{:S(2)}, u32[]{:S(2)}) collective-permute-start(bf16[512,512]{1,0:T(8,128)(2,1)S(1)} %get-tuple-element.66), channel_id=1, source_target_pairs={{0,48},{16,0},{32,16},{48,32},{64,112},{80,64},{96,80},{112,96},{1... | collective-permute-start | bytes 1572872 | tf_op jit(solution)/shard_map/ppermute | solution.py:391
  137.5 23.1 %collective-permute-start.29 = (bf16[512,512]{1,0:T(8,128)(2,1)S(1)}, bf16[512,512]{1,0:T(8,128)(2,1)S(1)}, u32[]{:S(2)}, u32[]{:S(2)}) collective-permute-start(bf16[512,512]{1,0:T(8,128)(2,1)S(1)} %get-tuple-element.67), channel_id=1, source_target_pairs={{0,32},{16,48},{32,0},{48,16},{64,96},{80,112},{96,64},{112,80},{1... | collective-permute-start | bytes 1572872 | tf_op jit(solution)/shard_map/ppermute | solution.py:391
  147.6 15.7 %collective-permute-start.30 = (bf16[512,512]{1,0:T(8,128)(2,1)S(1)}, bf16[512,512]{1,0:T(8,128)(2,1)S(1)}, u32[]{:S(2)}, u32[]{:S(2)}) collective-permute-start(bf16[512,512]{1,0:T(8,128)(2,1)S(1)} %get-tuple-element.68), channel_id=1, source_target_pairs={{0,16},{16,32},{32,48},{48,0},{64,80},{80,96},{96,112},{112,64},{1... | collective-permute-start | bytes 1572872 | tf_op jit(solution)/shard_map/ppermute | solution.py:391
  166.8 16.0 %collective-permute-start.31 = (bf16[512,512]{1,0:T(8,128)(2,1)S(1)}, bf16[512,512]{1,0:T(8,128)(2,1)S(1)}, u32[]{:S(2)}, u32[]{:S(2)}) collective-permute-start(bf16[512,512]{1,0:T(8,128)(2,1)S(1)} %get-tuple-element.70), channel_id=1, source_target_pairs={{0,48},{16,0},{32,16},{48,32},{64,112},{80,64},{96,80},{112,96},{1... | collective-permute-start | bytes 1572872 | tf_op jit(solution)/shard_map/ppermute | solution.py:391
  167.9 19.7 %collective-permute-start.32 = (bf16[512,512]{1,0:T(8,128)(2,1)S(1)}, bf16[512,512]{1,0:T(8,128)(2,1)S(1)}, u32[]{:S(2)}, u32[]{:S(2)}) collective-permute-start(bf16[512,512]{1,0:T(8,128)(2,1)S(1)} %get-tuple-element.71), channel_id=1, source_target_pairs={{0,16},{16,32},{32,48},{48,0},{64,80},{80,96},{96,112},{112,64},{1... | collective-permute-start | bytes 1572872 | tf_op jit(solution)/shard_map/ppermute | solution.py:391
  170.9 17.5 %collective-permute-start.33 = (bf16[512,512]{1,0:T(8,128)(2,1)S(1)}, bf16[512,512]{1,0:T(8,128)(2,1)S(1)}, u32[]{:S(2)}, u32[]{:S(2)}) collective-permute-start(bf16[512,512]{1,0:T(8,128)(2,1)S(1)} %get-tuple-element.72), channel_id=1, source_target_pairs={{0,32},{16,48},{32,0},{48,16},{64,96},{80,112},{96,64},{112,80},{1... | collective-permute-start | bytes 1572872 | tf_op jit(solution)/shard_map/ppermute | solution.py:391
  172.0 21.8 %collective-permute-start.34 = (bf16[512,512]{1,0:T(8,128)(2,1)S(1)}, bf16[512,512]{1,0:T(8,128)(2,1)S(1)}, u32[]{:S(2)}, u32[]{:S(2)}) collective-permute-start(bf16[512,512]{1,0:T(8,128)(2,1)S(1)} %get-tuple-element.74), channel_id=1, source_target_pairs={{0,192},{16,208},{32,224},{48,240},{64,0},{80,16},{96,32},{112,48}... | collective-permute-start | bytes 1572872 | tf_op jit(solution)/shard_map/ppermute | solution.py:391
  176.8 19.7 %collective-permute-start.35 = (bf16[512,512]{1,0:T(8,128)(2,1)S(1)}, bf16[512,512]{1,0:T(8,128)(2,1)S(1)}, u32[]{:S(2)}, u32[]{:S(2)}) collective-permute-start(bf16[512,512]{1,0:T(8,128)(2,1)S(1)} %get-tuple-element.75), channel_id=1, source_target_pairs={{0,64},{16,80},{32,96},{48,112},{64,128},{80,144},{96,160},{112,17... | collective-permute-start | bytes 1572872 | tf_op jit(solution)/shard_map/ppermute | solution.py:391
  (19 other events, 263.6 us)

commit v4 on v2

--- a/solution.py
+++ b/solution.py
@@ -235,7 +235,7 @@
         columns_ref[at, :] = jnp.broadcast_to(line, (slots, slots)).T
     last = (((1,), (1,)), ((), ()))
     units = gate_ref.shape[0]
-    width, rows = units // 4, 2 * slots
+    width, rows = units // 4, (4 if len(blocks) % 4 == 0 else number + 1) * slots
 
     def work(i, carry):
         at = pl.ds(pl.multiple_of(i * rows, rows), rows)
@@ -249,7 +249,7 @@
         result_ref[at, :] = (result * columns_ref[at, :][:, :1]).astype(jnp.bfloat16)
         return carry
 
-    lax.fori_loop(0, len(blocks) // 2, work, 0)
+    lax.fori_loop(0, len(blocks) * slots // rows, work, 0)
 
     def part(block, which):
         if block in blocks:
@@ -366,10 +366,10 @@
 
 def add(lows, highs):
     tokens, half = lows[0].shape
-    step = tokens // 4
+    step = tokens // 2
     return pl.pallas_call(
         add_kernel,
-        grid=(4,),
+        grid=(2,),
         in_specs=[pl.BlockSpec((step, half), lambda i: (i, 0))] * (2 * SIDE),
         out_specs=pl.BlockSpec((step, 2 * half), lambda i: (i, 0)),
         out_shape=jax.ShapeDtypeStruct((tokens, 2 * half), jnp.bfloat16),

time: 197 us -> 197 us (level)
  the two profiles are of different devices: /device:TPU:32 before, /device:TPU:36 now
where the time goes in v4:
time: 197 us; the launch traced here: 196 us
  waiting for transfers between devices  88.8 us (45%)
  starting transfers between devices  61.2 us (31%)
  Pallas kernels  34.8 us (18%)
  local copies, waits for them, and re-layouts  10.5 us (5%)
    ppermute x26, waiting for transfers between devices, over_plane(): lax.ppermute(array, 'ep', [(y * SIDE + x, (y + by_y) % SIDE * SIDE + (x +...  54.8 us
    ppermute x26, starting transfers between devices, over_plane(): lax.ppermute(array, 'ep', [(y * SIDE + x, (y + by_y) % SIDE * SIDE + (x +...  46.5 us
    ppermute x4, waiting for transfers between devices, along_z(): lax.ppermute(array, 'tp', [(z * 2 + c, to * 2 + c) for z, c, to in pairs])  26.7 us
    pallas_call x3, Pallas kernels, expert(): pl.pallas_call(functools.partial(expert_kernel, number, [*inputs, *outs])...  16.8 us
    ppermute x4, starting transfers between devices, along_z(): lax.ppermute(array, 'tp', [(z * 2 + c, to * 2 + c) for z, c, to in pairs])  8.3 us
    pallas_call x2, Pallas kernels, pick(): pl.pallas_call(functools.partial(pick_kernel, along_y), in_specs=[SMEM] +...  6.38 us
    all_to_all x1, starting transfers between devices, layer(): lax.all_to_all(rows_there, 'ep', split_axis=0, concat_axis=0, tiled=True)  6.24 us
    unnamed x16, local copies, waits for them, and re-layouts  5.72 us
  transfers between devices with their start and end apart: 36, of which 15 were waited for; matrix products, arithmetic and copies ran while one was open for 3% of the time, Pallas kernels for 7%

profile of v4, /device:TPU:36, one launch (start us, length us, event | category | flops | bytes accessed | tf_op | source)
XLA Modules:
  0.0 196.1 jit_solution(18036705319071550123)
XLA Ops:
  7.7 10.1 %collective-permute-done.1.refs_1_ = bf16[3,128,1024]{2,1,0:T(8,128)(2,1)S(1)} collective-permute-done((bf16[3,128,1024]{2,1,0:T(8,128)(2,1)S(1)}, bf16[3,128,1024]{2,1,0:T(8,128)(2,1)S(1)}, u32[]{:S(2)}, u32[]{:S(2)}) %collective-permute-start.1) | collective-permute-done | bytes 786464 | tf_op jit(solution)/shard_map/ppermute | solution.py:392
  24.9 6.7 %collective-permute-done.2.refs_2_ = bf16[3,128,1024]{2,1,0:T(8,128)(2,1)S(1)} collective-permute-done((bf16[3,128,1024]{2,1,0:T(8,128)(2,1)S(1)}, bf16[3,128,1024]{2,1,0:T(8,128)(2,1)S(1)}, u32[]{:S(2)}, u32[]{:S(2)}) %collective-permute-start.2) | collective-permute-done | bytes 786464 | tf_op jit(solution)/shard_map/ppermute | solution.py:392
  49.0 6.2 %all-to-all-start = ((s32[16,8,128]{2,1,0:T(8,128)}), s32[16,8,128]{2,1,0:T(8,128)S(1)}, u32[]{:S(2)}, u32[]{:S(2)}) async-start(s32[16,8,128]{2,1,0:T(8,128)} %get-tuple-element.40), calls=%async_computation | async-start | bytes 131072 | tf_op jit(solution)/shard_map/all_to_all | solution.py:413
  55.3 5.5 %all-to-all-done.rows_ref = s32[16,8,128]{2,1,0:T(8,128)S(1)} async-done(((s32[16,8,128]{2,1,0:T(8,128)}), s32[16,8,128]{2,1,0:T(8,128)S(1)}, u32[]{:S(2)}, u32[]{:S(2)}) %all-to-all-start) | async-done | bytes 65568 | tf_op jit(solution)/shard_map/all_to_all | solution.py:413
  68.1 4.3 %collective-permute-start.4 = (bf16[3,64,1024]{2,1,0:T(8,128)(2,1)S(1)}, bf16[3,64,1024]{2,1,0:T(8,128)(2,1)S(1)}, u32[]{:S(2)}, u32[]{:S(2)}) collective-permute-start(bf16[3,64,1024]{2,1,0:T(8,128)(2,1)S(1)} %slice.20), channel_id=1, source_target_pairs={{0,4},{1,13},{2,6},{3,15},{4,8},{5,1},{6,10},{7,3},{8,12},{9,5},{1... | collective-permute-start | bytes 1179656 | tf_op jit(solution)/shard_map/ppermute | solution.py:392
  72.4 9.9 %collective-permute-done.4.refs_4_ = bf16[3,64,1024]{2,1,0:T(8,128)(2,1)S(1)} collective-permute-done((bf16[3,64,1024]{2,1,0:T(8,128)(2,1)S(1)}, bf16[3,64,1024]{2,1,0:T(8,128)(2,1)S(1)}, u32[]{:S(2)}, u32[]{:S(2)}) %collective-permute-start.4) | collective-permute-done | bytes 393248 | tf_op jit(solution)/shard_map/ppermute | solution.py:392
  84.9 3.3 %pick_x.1 = (bf16[512,512]{1,0:T(8,128)(2,1)S(1)}, bf16[512,512]{1,0:T(8,128)(2,1)S(1)}, bf16[512,512]{1,0:T(8,128)(2,1)S(1)}, bf16[512,512]{1,0:T(8,128)(2,1)S(1)}) custom-call(s32[2]{0:T(128)S(1)} %pad_add_fusion.place_ref, s32[16,8,128]{2,1,0:T(8,128)S(1)} %all-to-all-done.rows_ref, bf16[512,512]{1,0:T(8,128)(2,1)S(1)} %copy-done.5, ...), custom_call_target="tpu_custom_call" | custom-call | flops 1073741824 | bytes 4194304 | tf_op jit(solution)/shard_map/pick_x/pallas_call | solution.py:142
  90.3 3.4 %collective-permute-start.22 = (bf16[512,512]{1,0:T(8,128)(2,1)S(1)}, bf16[512,512]{1,0:T(8,128)(2,1)S(1)}, u32[]{:S(2)}, u32[]{:S(2)}) collective-permute-start(bf16[512,512]{1,0:T(8,128)(2,1)S(1)} %get-tuple-element.56), channel_id=1, source_target_pairs={{0,32},{16,48},{32,0},{48,16},{64,96},{80,112},{96,64},{112,80},{1... | collective-permute-start | bytes 1572872 | tf_op jit(solution)/shard_map/ppermute | solution.py:384
  95.4 12.6 %collective-permute-done.14.refs_3_.refs_2_ = bf16[512,512]{1,0:T(8,128)(2,1)S(1)} collective-permute-done((bf16[512,512]{1,0:T(8,128)(2,1)S(1)}, bf16[512,512]{1,0:T(8,128)(2,1)S(1)}, u32[]{:S(2)}, u32[]{:S(2)}) %collective-permute-start.14) | collective-permute-done | bytes 524320 | tf_op jit(solution)/shard_map/ppermute | solution.py:384
  108.0 4.0 %shard_map.74 = (bf16[512,512]{1,0:T(8,128)(2,1)S(1)}, bf16[512,512]{1,0:T(8,128)(2,1)S(1)}) custom-call(s32[2]{0:T(128)S(1)} %pad_add_fusion.place_ref, f32[16,128]{1,0:T(8,128)S(1)} %copy-done.7, bf16[1024,1024]{1,0:T(8,128)(2,1)S(1)} %get-tuple-element.43.gate_ref, bf16[1024,1024]{1,0:T(8,128)(2,1)S(1)} %get-tuple-element.44.up_ref, ...), custom_call_target="tpu_custom_call" | custom-call | flops 3221225472 | bytes 2097152 | tf_op jit(solution)/shard_map/pallas_call | solution.py:296
  114.4 6.5 %shard_map.75 = (bf16[512,512]{1,0:T(8,128)(2,1)S(1)}, bf16[512,512]{1,0:T(8,128)(2,1)S(1)}, bf16[768,512]{1,0:T(8,128)(2,1)S(1)}, bf16[768,512]{1,0:T(8,128)(2,1)S(1)}) custom-call(s32[2]{0:T(128)S(1)} %pad_add_fusion.place_ref, f32[16,128]{1,0:T(8,128)S(1)} %copy-done.7, bf16[1024,1024]{1,0:T(8,128)(2,1)S(1)} %get-tuple-element.43.gate_ref, ...), custom_call_target="tpu_custom_call" | custom-call | flops 4831838208 | bytes 3145728 | tf_op jit(solution)/shard_map/pallas_call | solution.py:296
  120.9 6.3 %shard_map.76 = (bf16[512,512]{1,0:T(8,128)(2,1)S(1)}, bf16[512,512]{1,0:T(8,128)(2,1)S(1)}, bf16[512,512]{1,0:T(8,128)(2,1)S(1)}, bf16[512,512]{1,0:T(8,128)(2,1)S(1)}, bf16[512,512]{1,0:T(8,128)(2,1)S(1)}) custom-call(s32[2]{0:T(128)S(1)} %pad_add_fusion.place_ref, f32[16,128]{1,0:T(8,128)S(1)} %copy-done.7, ...), custom_call_target="tpu_custom_call" | custom-call | flops 4831838208 | bytes 3145728 | tf_op jit(solution)/shard_map/pallas_call | solution.py:296
  134.0 3.6 %collective-permute-start.27 = (bf16[512,512]{1,0:T(8,128)(2,1)S(1)}, bf16[512,512]{1,0:T(8,128)(2,1)S(1)}, u32[]{:S(2)}, u32[]{:S(2)}) collective-permute-start(bf16[512,512]{1,0:T(8,128)(2,1)S(1)} %get-tuple-element.65), channel_id=1, source_target_pairs={{0,32},{16,48},{32,0},{48,16},{64,96},{80,112},{96,64},{112,80},{1... | collective-permute-start | bytes 1572872 | tf_op jit(solution)/shard_map/ppermute | solution.py:384
  137.5 4.5 %collective-permute-done.23.refs_1_ = bf16[512,512]{1,0:T(8,128)(2,1)S(1)} collective-permute-done((bf16[512,512]{1,0:T(8,128)(2,1)S(1)}, bf16[512,512]{1,0:T(8,128)(2,1)S(1)}, u32[]{:S(2)}, u32[]{:S(2)}) %collective-permute-start.23) | collective-permute-done | bytes 524320 | tf_op jit(solution)/shard_map/ppermute | solution.py:384
  142.0 3.6 %collective-permute-start.28 = (bf16[512,512]{1,0:T(8,128)(2,1)S(1)}, bf16[512,512]{1,0:T(8,128)(2,1)S(1)}, u32[]{:S(2)}, u32[]{:S(2)}) collective-permute-start(bf16[512,512]{1,0:T(8,128)(2,1)S(1)} %get-tuple-element.66), channel_id=1, source_target_pairs={{0,16},{16,32},{32,48},{48,0},{64,80},{80,96},{96,112},{112,64},{1... | collective-permute-start | bytes 1572872 | tf_op jit(solution)/shard_map/ppermute | solution.py:384
  145.6 9.0 %collective-permute-done.25.refs_3_ = bf16[512,512]{1,0:T(8,128)(2,1)S(1)} collective-permute-done((bf16[512,512]{1,0:T(8,128)(2,1)S(1)}, bf16[512,512]{1,0:T(8,128)(2,1)S(1)}, u32[]{:S(2)}, u32[]{:S(2)}) %collective-permute-start.25) | collective-permute-done | bytes 524320 | tf_op jit(solution)/shard_map/ppermute | solution.py:384
  154.6 3.9 %collective-permute-done.28.refs_7_ = bf16[512,512]{1,0:T(8,128)(2,1)S(1)} collective-permute-done((bf16[512,512]{1,0:T(8,128)(2,1)S(1)}, bf16[512,512]{1,0:T(8,128)(2,1)S(1)}, u32[]{:S(2)}, u32[]{:S(2)}) %collective-permute-start.28) | collective-permute-done | bytes 524320 | tf_op jit(solution)/shard_map/ppermute | solution.py:384
  158.5 3.4 %relay.1 = (bf16[512,512]{1,0:T(8,128)(2,1)S(1)}, bf16[512,512]{1,0:T(8,128)(2,1)S(1)}, bf16[512,512]{1,0:T(8,128)(2,1)S(1)}, bf16[512,512]{1,0:T(8,128)(2,1)S(1...) custom-call(s32[2]{0:T(128)S(1)} %pad_add_fusion.place_ref, ...), custom_call_target="tpu_custom_call" | custom-call | flops 2147483648 | bytes 8388608 | tf_op jit(solution)/shard_map/relay/pallas_call | solution.py:345
  164.8 4.5 %collective-permute-start.31 = (bf16[512,512]{1,0:T(8,128)(2,1)S(1)}, bf16[512,512]{1,0:T(8,128)(2,1)S(1)}, u32[]{:S(2)}, u32[]{:S(2)}) collective-permute-start(bf16[512,512]{1,0:T(8,128)(2,1)S(1)} %get-tuple-element.70), channel_id=1, source_target_pairs={{0,32},{16,48},{32,0},{48,16},{64,96},{80,112},{96,64},{112,80},{1... | collective-permute-start | bytes 1572872 | tf_op jit(solution)/shard_map/ppermute | solution.py:384
  169.3 4.3 %collective-permute-start.32 = (bf16[512,512]{1,0:T(8,128)(2,1)S(1)}, bf16[512,512]{1,0:T(8,128)(2,1)S(1)}, u32[]{:S(2)}, u32[]{:S(2)}) collective-permute-start(bf16[512,512]{1,0:T(8,128)(2,1)S(1)} %get-tuple-element.72), channel_id=1, source_target_pairs={{0,192},{16,208},{32,224},{48,240},{64,0},{80,16},{96,32},{112,48}... | collective-permute-start | bytes 1572872 | tf_op jit(solution)/shard_map/ppermute | solution.py:384
  173.5 3.9 %collective-permute-done.29.refs_1_ = bf16[512,512]{1,0:T(8,128)(2,1)S(1)} collective-permute-done((bf16[512,512]{1,0:T(8,128)(2,1)S(1)}, bf16[512,512]{1,0:T(8,128)(2,1)S(1)}, u32[]{:S(2)}, u32[]{:S(2)}) %collective-permute-start.29) | collective-permute-done | bytes 524320 | tf_op jit(solution)/shard_map/ppermute | solution.py:384
  178.8 7.9 %collective-permute-done.30.refs_2_ = bf16[512,512]{1,0:T(8,128)(2,1)S(1)} collective-permute-done((bf16[512,512]{1,0:T(8,128)(2,1)S(1)}, bf16[512,512]{1,0:T(8,128)(2,1)S(1)}, u32[]{:S(2)}, u32[]{:S(2)}) %collective-permute-start.30) | collective-permute-done | bytes 524320 | tf_op jit(solution)/shard_map/ppermute | solution.py:384
  186.8 4.7 %collective-permute-done.32.refs_5_ = bf16[512,512]{1,0:T(8,128)(2,1)S(1)} collective-permute-done((bf16[512,512]{1,0:T(8,128)(2,1)S(1)}, bf16[512,512]{1,0:T(8,128)(2,1)S(1)}, u32[]{:S(2)}, u32[]{:S(2)}) %collective-permute-start.32) | collective-permute-done | bytes 524320 | tf_op jit(solution)/shard_map/ppermute | solution.py:384
  191.5 3.3 %collective-permute-done.33.refs_6_ = bf16[512,512]{1,0:T(8,128)(2,1)S(1)} collective-permute-done((bf16[512,512]{1,0:T(8,128)(2,1)S(1)}, bf16[512,512]{1,0:T(8,128)(2,1)S(1)}, u32[]{:S(2)}, u32[]{:S(2)}) %collective-permute-start.33) | collective-permute-done | bytes 524320 | tf_op jit(solution)/shard_map/ppermute | solution.py:384
  (82 shorter events, 60.6 us)
Async XLA Ops:
  21.7 17.7 %collective-permute-start.15 = (bf16[512,512]{1,0:T(8,128)(2,1)}, bf16[512,512]{1,0:T(8,128)(2,1)}, u32[]{:S(2)}, u32[]{:S(2)}) collective-permute-start(bf16[512,512]{1,0:T(8,128)(2,1)} %get-tuple-element.50.own_ref), channel_id=1, source_target_pairs={{0,64},{16,80},{32,96},{48,112},{64,128},{80,144},{96,160},{112,17... | collective-permute-start | bytes 1572872 | tf_op jit(solution)/shard_map/ppermute | solution.py:384
  23.2 19.3 %collective-permute-start.17 = (bf16[512,512]{1,0:T(8,128)(2,1)}, bf16[512,512]{1,0:T(8,128)(2,1)}, u32[]{:S(2)}, u32[]{:S(2)}) collective-permute-start(bf16[512,512]{1,0:T(8,128)(2,1)} %get-tuple-element.50.own_ref), channel_id=1, source_target_pairs={{0,192},{16,208},{32,224},{48,240},{64,0},{80,16},{96,32},{112,48}... | collective-permute-start | bytes 1572872 | tf_op jit(solution)/shard_map/ppermute | solution.py:384
  31.6 40.7 %collective-permute-start.3 = (bf16[3,128,1024]{2,1,0:T(8,128)(2,1)S(1)}, bf16[3,128,1024]{2,1,0:T(8,128)(2,1)S(1)}, u32[]{:S(2)}, u32[]{:S(2)}) collective-permute-start(bf16[3,128,1024]{2,1,0:T(8,128)(2,1)S(1)} %collective-permute-done.2.refs_2_), channel_id=1, source_target_pairs={{0,2},{1,15},{2,4},{3,1},{4,6},{5,3},{6,8},{7,5},{8,10},{9,7},{10,... | collective-permute-start | bytes 2359304 | tf_op jit(solution)/shard_map/ppermute | solution.py:392
  38.5 22.3 %collective-permute-start.12 = (bf16[256,512]{1,0:T(8,128)(2,1)}, bf16[256,512]{1,0:T(8,128)(2,1)}, u32[]{:S(2)}, u32[]{:S(2)}) collective-permute-start(bf16[256,512]{1,0:T(8,128)(2,1)} %slice.22), channel_id=1, source_target_pairs={{0,48},{16,0},{32,16},{48,32},{64,112},{80,64},{96,80},{112,96},{1... | collective-permute-start | bytes 786440 | tf_op jit(solution)/shard_map/ppermute | solution.py:384
  41.0 26.9 %collective-permute-start.16 = (bf16[256,512]{1,0:T(8,128)(2,1)}, bf16[256,512]{1,0:T(8,128)(2,1)S(1)}, u32[]{:S(2)}, u32[]{:S(2)}) collective-permute-start(bf16[256,512]{1,0:T(8,128)(2,1)} %slice.23), channel_id=1, source_target_pairs={{0,64},{16,80},{32,96},{48,112},{64,128},{80,144},{96,160},{112,17... | collective-permute-start | bytes 786440 | tf_op jit(solution)/shard_map/ppermute | solution.py:384
  44.2 23.8 %collective-permute-start.18 = (bf16[256,512]{1,0:T(8,128)(2,1)}, bf16[256,512]{1,0:T(8,128)(2,1)}, u32[]{:S(2)}, u32[]{:S(2)}) collective-permute-start(bf16[256,512]{1,0:T(8,128)(2,1)} %slice.24), channel_id=1, source_target_pairs={{0,192},{16,208},{32,224},{48,240},{64,0},{80,16},{96,32},{112,48}... | collective-permute-start | bytes 786440 | tf_op jit(solution)/shard_map/ppermute | solution.py:384
  45.9 39.0 %collective-permute-start.5 = (bf16[3,128,1024]{2,1,0:T(8,128)(2,1)S(1)}, bf16[3,128,1024]{2,1,0:T(8,128)(2,1)}, u32[]{:S(2)}, u32[]{:S(2)}) collective-permute-start(bf16[3,128,1024]{2,1,0:T(8,128)(2,1)S(1)} %collective-permute-done.1.refs_1_), channel_id=1, source_target_pairs={{0,1},{1,0},{2,3},{3,2},{4,5},{5,4},{6,7},{7,6},{8,9},{9,8},{10,11... | collective-permute-start | bytes 2359304 | tf_op jit(solution)/shard_map/ppermute | solution.py:396
  68.0 20.3 %collective-permute-start.6 = (bf16[3,128,1024]{2,1,0:T(8,128)(2,1)S(1)}, bf16[3,128,1024]{2,1,0:T(8,128)(2,1)S(1)}, u32[]{:S(2)}, u32[]{:S(2)}) collective-permute-start(bf16[3,128,1024]{2,1,0:T(8,128)(2,1)S(1)} %collective-permute-done.2.refs_2_), channel_id=1, source_target_pairs={{0,1},{1,0},{2,3},{3,2},{4,5},{5,4},{6,7},{7,6},{8,9},{9,8},{10,11... | collective-permute-start | bytes 2359304 | tf_op jit(solution)/shard_map/ppermute | solution.py:396
  72.4 18.0 %collective-permute-start.7 = (bf16[3,128,1024]{2,1,0:T(8,128)(2,1)S(1)}, bf16[3,128,1024]{2,1,0:T(8,128)(2,1)S(1)}, u32[]{:S(2)}, u32[]{:S(2)}) collective-permute-start(bf16[3,128,1024]{2,1,0:T(8,128)(2,1)S(1)} %collective-permute-done.3.refs_3_), channel_id=1, source_target_pairs={{0,1},{1,0},{2,3},{3,2},{4,5},{5,4},{6,7},{7,6},{8,9},{9,8},{10,11... | collective-permute-start | bytes 2359304 | tf_op jit(solution)/shard_map/ppermute | solution.py:396
  82.2 25.8 %collective-permute-start.14 = (bf16[512,512]{1,0:T(8,128)(2,1)S(1)}, bf16[512,512]{1,0:T(8,128)(2,1)S(1)}, u32[]{:S(2)}, u32[]{:S(2)}) collective-permute-start(bf16[512,512]{1,0:T(8,128)(2,1)S(1)} %get-tuple-element.49), channel_id=1, source_target_pairs={{0,192},{16,208},{32,224},{48,240},{64,0},{80,16},{96,32},{112,48}... | collective-permute-start | bytes 1572872 | tf_op jit(solution)/shard_map/ppermute | solution.py:384
  84.9 23.1 %collective-permute-start.21 = (bf16[512,512]{1,0:T(8,128)(2,1)S(1)}, bf16[512,512]{1,0:T(8,128)(2,1)S(1)}, u32[]{:S(2)}, u32[]{:S(2)}) collective-permute-start(bf16[512,512]{1,0:T(8,128)(2,1)S(1)} %get-tuple-element.53), channel_id=1, source_target_pairs={{0,128},{16,144},{32,160},{48,176},{64,192},{80,208},{96,224},{112... | collective-permute-start | bytes 1572872 | tf_op jit(solution)/shard_map/ppermute | solution.py:384
  88.2 23.8 %collective-permute-start.19 = (bf16[512,512]{1,0:T(8,128)(2,1)S(1)}, bf16[512,512]{1,0:T(8,128)(2,1)S(1)}, u32[]{:S(2)}, u32[]{:S(2)}) collective-permute-start(bf16[512,512]{1,0:T(8,128)(2,1)S(1)} %get-tuple-element.51), channel_id=1, source_target_pairs={{0,16},{16,32},{32,48},{48,0},{64,80},{80,96},{96,112},{112,64},{1... | collective-permute-start | bytes 1572872 | tf_op jit(solution)/shard_map/ppermute | solution.py:384
  89.6 22.4 %collective-permute-start.20 = (bf16[512,512]{1,0:T(8,128)(2,1)S(1)}, bf16[512,512]{1,0:T(8,128)(2,1)S(1)}, u32[]{:S(2)}, u32[]{:S(2)}) collective-permute-start(bf16[512,512]{1,0:T(8,128)(2,1)S(1)} %get-tuple-element.52), channel_id=1, source_target_pairs={{0,48},{16,0},{32,16},{48,32},{64,112},{80,64},{96,80},{112,96},{1... | collective-permute-start | bytes 1572872 | tf_op jit(solution)/shard_map/ppermute | solution.py:384
  90.3 24.0 %collective-permute-start.22 = (bf16[512,512]{1,0:T(8,128)(2,1)S(1)}, bf16[512,512]{1,0:T(8,128)(2,1)S(1)}, u32[]{:S(2)}, u32[]{:S(2)}) collective-permute-start(bf16[512,512]{1,0:T(8,128)(2,1)S(1)} %get-tuple-element.56), channel_id=1, source_target_pairs={{0,32},{16,48},{32,0},{48,16},{64,96},{80,112},{96,64},{112,80},{1... | collective-permute-start | bytes 1572872 | tf_op jit(solution)/shard_map/ppermute | solution.py:384
  129.0 16.6 %collective-permute-start.24 = (bf16[512,512]{1,0:T(8,128)(2,1)S(1)}, bf16[512,512]{1,0:T(8,128)(2,1)S(1)}, u32[]{:S(2)}, u32[]{:S(2)}) collective-permute-start(bf16[512,512]{1,0:T(8,128)(2,1)S(1)} %get-tuple-element.61), channel_id=1, source_target_pairs={{0,128},{16,144},{32,160},{48,176},{64,192},{80,208},{96,224},{112... | collective-permute-start | bytes 1572872 | tf_op jit(solution)/shard_map/ppermute | solution.py:384
  130.6 24.0 %collective-permute-start.25 = (bf16[512,512]{1,0:T(8,128)(2,1)S(1)}, bf16[512,512]{1,0:T(8,128)(2,1)S(1)}, u32[]{:S(2)}, u32[]{:S(2)}) collective-permute-start(bf16[512,512]{1,0:T(8,128)(2,1)S(1)} %get-tuple-element.62), channel_id=1, source_target_pairs={{0,64},{16,80},{32,96},{48,112},{64,128},{80,144},{96,160},{112,17... | collective-permute-start | bytes 1572872 | tf_op jit(solution)/shard_map/ppermute | solution.py:384
  131.9 22.7 %collective-permute-start.26 = (bf16[512,512]{1,0:T(8,128)(2,1)S(1)}, bf16[512,512]{1,0:T(8,128)(2,1)S(1)}, u32[]{:S(2)}, u32[]{:S(2)}) collective-permute-start(bf16[512,512]{1,0:T(8,128)(2,1)S(1)} %get-tuple-element.64), channel_id=1, source_target_pairs={{0,48},{16,0},{32,16},{48,32},{64,112},{80,64},{96,80},{112,96},{1... | collective-permute-start | bytes 1572872 | tf_op jit(solution)/shard_map/ppermute | solution.py:384
  134.0 20.6 %collective-permute-start.27 = (bf16[512,512]{1,0:T(8,128)(2,1)S(1)}, bf16[512,512]{1,0:T(8,128)(2,1)S(1)}, u32[]{:S(2)}, u32[]{:S(2)}) collective-permute-start(bf16[512,512]{1,0:T(8,128)(2,1)S(1)} %get-tuple-element.65), channel_id=1, source_target_pairs={{0,32},{16,48},{32,0},{48,16},{64,96},{80,112},{96,64},{112,80},{1... | collective-permute-start | bytes 1572872 | tf_op jit(solution)/shard_map/ppermute | solution.py:384
  142.0 16.5 %collective-permute-start.28 = (bf16[512,512]{1,0:T(8,128)(2,1)S(1)}, bf16[512,512]{1,0:T(8,128)(2,1)S(1)}, u32[]{:S(2)}, u32[]{:S(2)}) collective-permute-start(bf16[512,512]{1,0:T(8,128)(2,1)S(1)} %get-tuple-element.66), channel_id=1, source_target_pairs={{0,16},{16,32},{32,48},{48,0},{64,80},{80,96},{96,112},{112,64},{1... | collective-permute-start | bytes 1572872 | tf_op jit(solution)/shard_map/ppermute | solution.py:384
  164.6 22.2 %collective-permute-start.30 = (bf16[512,512]{1,0:T(8,128)(2,1)S(1)}, bf16[512,512]{1,0:T(8,128)(2,1)S(1)}, u32[]{:S(2)}, u32[]{:S(2)}) collective-permute-start(bf16[512,512]{1,0:T(8,128)(2,1)S(1)} %get-tuple-element.69), channel_id=1, source_target_pairs={{0,16},{16,32},{32,48},{48,0},{64,80},{80,96},{96,112},{112,64},{1... | collective-permute-start | bytes 1572872 | tf_op jit(solution)/shard_map/ppermute | solution.py:384
  164.8 22.0 %collective-permute-start.31 = (bf16[512,512]{1,0:T(8,128)(2,1)S(1)}, bf16[512,512]{1,0:T(8,128)(2,1)S(1)}, u32[]{:S(2)}, u32[]{:S(2)}) collective-permute-start(bf16[512,512]{1,0:T(8,128)(2,1)S(1)} %get-tuple-element.70), channel_id=1, source_target_pairs={{0,32},{16,48},{32,0},{48,16},{64,96},{80,112},{96,64},{112,80},{1... | collective-permute-start | bytes 1572872 | tf_op jit(solution)/shard_map/ppermute | solution.py:384
  169.3 22.2 %collective-permute-start.32 = (bf16[512,512]{1,0:T(8,128)(2,1)S(1)}, bf16[512,512]{1,0:T(8,128)(2,1)S(1)}, u32[]{:S(2)}, u32[]{:S(2)}) collective-permute-start(bf16[512,512]{1,0:T(8,128)(2,1)S(1)} %get-tuple-element.72), channel_id=1, source_target_pairs={{0,192},{16,208},{32,224},{48,240},{64,0},{80,16},{96,32},{112,48}... | collective-permute-start | bytes 1572872 | tf_op jit(solution)/shard_map/ppermute | solution.py:384
  173.5 21.3 %collective-permute-start.33 = (bf16[512,512]{1,0:T(8,128)(2,1)S(1)}, bf16[512,512]{1,0:T(8,128)(2,1)S(1)}, u32[]{:S(2)}, u32[]{:S(2)}) collective-permute-start(bf16[512,512]{1,0:T(8,128)(2,1)S(1)} %get-tuple-element.73), channel_id=1, source_target_pairs={{0,64},{16,80},{32,96},{48,112},{64,128},{80,144},{96,160},{112,17... | collective-permute-start | bytes 1572872 | tf_op jit(solution)/shard_map/ppermute | solution.py:384
  177.5 17.3 %collective-permute-start.34 = (bf16[512,512]{1,0:T(8,128)(2,1)S(1)}, bf16[512,512]{1,0:T(8,128)(2,1)S(1)}, u32[]{:S(2)}, u32[]{:S(2)}) collective-permute-start(bf16[512,512]{1,0:T(8,128)(2,1)S(1)} %get-tuple-element.74), channel_id=1, source_target_pairs={{0,128},{16,144},{32,160},{48,176},{64,192},{80,208},{96,224},{112... | collective-permute-start | bytes 1572872 | tf_op jit(solution)/shard_map/ppermute | solution.py:384
  (20 other events, 192.2 us)
